TPU v7x, 128 devices: a whole 4x4x4 slice. The times are simulated.
128 devices in a mesh: sp: 16 (over z, x), tp: 8 (over y, core).
Axes of the slice: x: 4, y: 4, z: 4, core: 2. Of those that a mesh axis runs over, the one named last changes fastest.
Arguments:
- tokens: bfloat16 [4, 16384, 2048], P(None, 'sp'), may hold values from -6 to 6
- norm_gain: bfloat16 [2048], replicated, may hold values from 0.099609375 to 1.8984375
- conv_value_weight: bfloat16 [2048, 1024], P('sp', 'tp'), may hold values from -0.125 to 0.125
- conv_gate_weight: bfloat16 [2048, 1024], P('sp', 'tp'), may hold values from -0.125 to 0.125
- query_weight: bfloat16 [2048, 1024], P('sp', 'tp'), may hold values from -40 to 40
- key_weight: bfloat16 [2048, 512], P('sp', 'tp'), may hold values from -1 to 1
- value_weight: bfloat16 [2048, 512], P('sp', 'tp'), may hold values from -0.125 to 0.125
- conv_taps: bfloat16 [31, 1024], P(None, 'tp'), may hold values from -1 to 1
- conv_gain: bfloat16 [1024], P('tp'), may hold values from 0.099609375 to 1.8984375
- sink_logit: float32 [16], P('tp'), may hold values from 1 to 6
- out_conv_weight: bfloat16 [1024, 2048], P('tp', 'sp'), may hold values from -0.125 to 0.125
- out_attn_weight: bfloat16 [1024, 2048], P('tp', 'sp'), may hold values from -0.125 to 0.125
Outputs:
- mixed: bfloat16 [4, 16384, 2048], P(None, ('sp', 'tp'))
- log_total: float32 [4, 16, 16384], P(None, 'tp', 'sp')
All inputs are finite; a program needn't handle non-finite values.
Results may differ from a plain program's by a relative error of at most 0.015.
Values may be sent and summed in bfloat16 or wider, within the bound.
A program may use at most 128 MiB of HBM per device.

v0:
```python
import functools

import jax
import jax.numpy as jnp
from jax import lax
from jax.experimental import pallas as pl
from jax.experimental.pallas import tpu as pltpu
from jax.sharding import PartitionSpec as P

MESH = pl.DeviceIdType.MESH
F32 = jnp.float32
BF16 = jnp.bfloat16

HEAD_DIM = 64
WINDOW = 128
EPSILON = 1e-06
ROPE_BASE = 10000.0
MASK_VALUE = -1e30
RIM = 16
LN_ROWS = 256
CORES = 2


def dot(a, b, dims=((1,), (0,))):
    return lax.dot_general(a, b, (dims, ((), ())), preferred_element_type=F32)


def kernel(
    dims,
    tokens,
    norm_gain,
    w_value,
    w_gate,
    w_query,
    w_key,
    w_val,
    conv_taps,
    conv_gain,
    sink,
    w_oc,
    w_oa,
    cos_ref,
    sin_ref,
    mixed,
    log_total,
    tbuf,
    gain_buf,
    normed,
    w_a,
    w_b,
    o_w,
    gain_all,
    taps_buf,
    gpad,
    qz,
    kpad,
    kvpad,
    bias,
    fsend,
    asend,
    cbm,
    bm,
    tok_sem,
    send_sem,
    recv_sem,
):
    SEQS, T, D, X, Z, Y, TP = dims
    NSP = X * Z
    per_seq = T // LN_ROWS
    n_blocks = SEQS * per_seq
    sp, tp = lax.axis_index("sp"), lax.axis_index("tp")
    z, x = sp // X, sp % X
    y, c = tp // CORES, tp % CORES
    half_y = Y // 2
    yh, yl = y // half_y, y % half_y
    slot = c * Y + y

    def at_x(d):
        return (z * X + (x + d) % X, tp)

    def at_z(d):
        return (((z + d) % Z) * X + x, tp)

    def at_y(d):
        return (sp, ((y + d) % Y) * CORES + c)

    def at_tp(d):
        return (sp, (tp + d) % TP)

    partner = (sp, y * CORES + (1 - c))
    right = ((sp + 1) % NSP, tp)
    left = ((sp + NSP - 1) % NSP, tp)

    counter = [0]

    def ids(n):
        first = counter[0]
        counter[0] += n
        return first

    def remote(src, dst, i, device):
        return pltpu.make_async_remote_copy(
            src_ref=src,
            dst_ref=dst,
            send_sem=send_sem.at[i],
            recv_sem=recv_sem.at[i],
            device_id=device,
            device_id_type=MESH,
        )

    def start(copies):
        for cp in copies:
            cp.start()

    def arrived(copies):
        for cp in copies:
            cp.wait_recv()

    def tok_copy(i):
        s, r = i // per_seq, (i % per_seq) * LN_ROWS
        return pltpu.make_async_copy(
            tokens.at[s, pl.ds(pl.multiple_of(r, LN_ROWS), LN_ROWS)], tbuf.at[i % 3], tok_sem.at[i % 3]
        )

    tok_copy(0).start()
    tok_copy(1).start()

    barrier = pltpu.get_barrier_semaphore()
    greeted = (
        [at_x(d) for d in range(1, X)]
        + [at_z(d) for d in range(1, Z)]
        + [left, right]
        + [at_tp(d) for d in range(1, TP)]
    )
    for device in greeted:
        pl.semaphore_signal(barrier, inc=1, device_id=device, device_id_type=MESH)

    w_a[z, x] = jnp.concatenate([w_value[...], w_gate[...]], axis=1)
    w_b[z, x] = jnp.concatenate([w_query[...], w_key[...], w_val[...]], axis=1)
    o_w[c, yh, z, x, pl.ds(pl.multiple_of(yl * 256, 256), 256)] = jnp.concatenate(
        [w_oc[...], w_oa[...]], axis=0
    )
    gain_all[slot] = jnp.broadcast_to(conv_gain[...].astype(F32), (8, 128))
    taps_buf[...] = conv_taps[...].astype(F32)
    gain_buf[...] = jnp.broadcast_to(norm_gain[...].astype(F32), (16, D))
    key_i = lax.broadcasted_iota(jnp.int32, (WINDOW, 256), 0)
    query_i = lax.broadcasted_iota(jnp.int32, (WINDOW, 256), 1) % WINDOW
    bias[0] = jnp.where(key_i >= query_i, 0.0, MASK_VALUE)
    bias[1] = jnp.where(key_i <= query_i, 0.0, MASK_VALUE)

    i = ids(X - 1)
    in_1 = [remote(w_a.at[z, x], w_a.at[z, x], i + d - 1, at_x(d)) for d in range(1, X)]
    i = ids(Z - 1)
    in_1 += [remote(w_b.at[z, x], w_b.at[z, x], i + d - 1, at_z(d)) for d in range(1, Z)]
    i = ids(Z - 1)
    in_2 = [remote(w_a.at[z], w_a.at[z], i + d - 1, at_z(d)) for d in range(1, Z)]
    i = ids(X - 1)
    in_2 += [remote(w_b.at[:, x], w_b.at[:, x], i + d - 1, at_x(d)) for d in range(1, X)]
    i = ids(Y - 1)
    tile = o_w.at[c, yh, z, x, pl.ds(pl.multiple_of(yl * 256, 256), 256)]
    out_0 = [remote(tile, tile, i + d - 1, at_y(d)) for d in range(1, Y)]
    i = ids(TP - 1)
    gains = [remote(gain_all.at[slot], gain_all.at[slot], i + d - 1, at_tp(d)) for d in range(1, TP)]
    i = ids(X - 1)
    out_1 = [remote(o_w.at[c, 0, z, x], o_w.at[c, 0, z, x], i + d - 1, at_x(d)) for d in range(1, X)]
    i = ids(Z - 1)
    out_1 += [remote(o_w.at[c, 1, z, x], o_w.at[c, 1, z, x], i + d - 1, at_z(d)) for d in range(1, Z)]
    i = ids(Z - 1)
    out_2 = [remote(o_w.at[c, 0, z], o_w.at[c, 0, z], i + d - 1, at_z(d)) for d in range(1, Z)]
    i = ids(X - 1)
    out_2 += [remote(o_w.at[c, 1, :, x], o_w.at[c, 1, :, x], i + d - 1, at_x(d)) for d in range(1, X)]
    i = ids(2)
    pair_1 = [
        remote(o_w.at[c, 0, z], o_w.at[c, 0, z], i, partner),
        remote(o_w.at[c, 1, :, x], o_w.at[c, 1, :, x], i + 1, partner),
    ]
    i = ids(Z - 1)
    pair_2 = []
    for d in range(1, Z):
        row = o_w.at[c, 0, (z + Z - d) % Z]
        pair_2.append(remote(row, row, i + d - 1, partner))
    i = ids(X - 1)
    for d in range(1, X):
        column = o_w.at[c, 1, :, (x + X - d) % X]
        pair_2.append(remote(column, column, i + d - 1, partner))

    halo_i = ids(4 * SEQS)

    def halos(s):
        i = halo_i + 4 * s
        return [
            remote(gpad.at[s, pl.ds(RIM, RIM)], gpad.at[s, pl.ds(RIM + T, RIM)], i, left),
            remote(gpad.at[s, pl.ds(T, RIM)], gpad.at[s, pl.ds(0, RIM)], i + 1, right),
            remote(kvpad.at[s, pl.ds(WINDOW, WINDOW)], kvpad.at[s, pl.ds(WINDOW + T, WINDOW)], i + 2, left),
            remote(kvpad.at[s, pl.ds(T, WINDOW)], kvpad.at[s, pl.ds(0, WINDOW)], i + 3, right),
        ]

    conv_i = ids((TP - 1) * SEQS)
    attn_i = ids((TP - 1) * SEQS)

    def rows_of(device_tp):
        return pl.ds(pl.multiple_of(device_tp * 128, 128), 128)

    conv_lanes = pl.ds(pl.multiple_of(slot * 128, 128), 128)
    attn_lanes = pl.ds(pl.multiple_of(slot * 256 + 128, 128), 128)

    def conv_out_copies(s):
        return [
            remote(
                fsend.at[s, rows_of((tp + d) % TP)],
                cbm.at[s, :, conv_lanes],
                conv_i + (TP - 1) * s + d - 1,
                at_tp(d),
            )
            for d in range(1, TP)
        ]

    def attn_out_copies(s):
        return [
            remote(
                asend.at[s, rows_of((tp + d) % TP)],
                bm.at[s, :, attn_lanes],
                attn_i + (TP - 1) * s + d - 1,
                at_tp(d),
            )
            for d in range(1, TP)
        ]

    pl.semaphore_wait(barrier, len(greeted))
    start(in_1)
    start(out_0)
    start(gains)

    def ln_block(i, carry):
        buf = i % 3
        tok_copy(i).wait()

        @pl.when(i + 2 < n_blocks)
        def _():
            tok_copy(i + 2).start()

        def group(g, carry):
            at = pl.multiple_of(g * 16, 16)
            v = tbuf[buf, pl.ds(at, 16), :].astype(F32)
            mean = jnp.sum(v, axis=-1, keepdims=True) * (1.0 / D)
            centred = v - mean
            var = jnp.sum(centred * centred, axis=-1, keepdims=True) * (1.0 / D)
            out = centred * lax.rsqrt(var + EPSILON) * gain_buf[...]
            normed[pl.ds(pl.multiple_of(i * LN_ROWS, LN_ROWS) + at, 16), :] = out.astype(BF16)
            return carry

        return lax.fori_loop(0, LN_ROWS // 16, group, carry, unroll=4)

    first_part = n_blocks // 4
    lax.fori_loop(0, first_part, ln_block, 0)
    arrived(in_1)
    start(in_2)
    lax.fori_loop(first_part, n_blocks, ln_block, 0)
    arrived(in_2)
    arrived(out_0)
    start(out_1)

    lane = lax.broadcasted_iota(jnp.int32, (1, 128), 1)
    low_half = (lane % HEAD_DIM) < HEAD_DIM // 2
    low_head = lane < HEAD_DIM

    def swapped(v):
        return jnp.where(low_half, pltpu.roll(v, 96, 1), pltpu.roll(v, 32, 1))

    proj_rows = 256

    def project(s):
        def step(k, carry):
            r = pl.multiple_of(k * proj_rows, proj_rows)
            rows = normed[pl.ds(pl.multiple_of(s * T, T) + r, proj_rows), :]
            a = dot(rows, w_a[...].reshape(D, 256))
            gated = a[:, :128] * jax.nn.sigmoid(a[:, 128:])
            gpad[s, pl.ds(RIM + r, proj_rows), :] = gated.astype(BF16).astype(F32)
            b = dot(rows, w_b[...].reshape(D, 256))
            cosine = cos_ref[pl.ds(r, proj_rows), :]
            sine = sin_ref[pl.ds(r, proj_rows), :]
            q, kv = b[:, :128], b[:, 128:]
            q = (q * cosine + swapped(q) * sine) * (HEAD_DIM**-0.5)
            zero = jnp.zeros_like(q)
            q_0 = jnp.where(low_head, q, zero).astype(BF16)
            q_1 = jnp.where(low_head, zero, q).astype(BF16)
            for n in range(proj_rows // 128):
                blk = k * (proj_rows // 128) + n
                qz[s, blk, 0] = q_0[n * 128 : (n + 1) * 128]
                qz[s, blk, 1] = q_1[n * 128 : (n + 1) * 128]
            turned = kv * cosine + swapped(kv) * sine
            kpad[s, pl.ds(WINDOW + r, proj_rows), :] = jnp.where(
                low_head, turned, pltpu.roll(turned, 64, 1)
            ).astype(BF16)
            kvpad[s, pl.ds(WINDOW + r, proj_rows), :] = jnp.where(low_head, turned, kv).astype(BF16)
            return carry

        lax.fori_loop(0, T // proj_rows, step, 0)

    def convolve(s):
        arriving = halos(s)
        arriving[0].wait_recv()
        arriving[1].wait_recv()

        @pl.when(sp == 0)
        def _():
            gpad[s, pl.ds(0, RIM), :] = jnp.zeros((RIM, 128), F32)

        @pl.when(sp == NSP - 1)
        def _():
            gpad[s, pl.ds(RIM + T, RIM), :] = jnp.zeros((RIM, 128), F32)

        def chunk(k, carry):
            r = pl.multiple_of(k * 128, 128)
            total = jnp.zeros((128, 128), F32)
            for j in range(31):
                total = total + gpad[s, pl.ds(r + (j + 1), 128), :] * taps_buf[pl.ds(j, 1), :]
            fsend[s, pl.ds(r, 128), :] = total.astype(BF16)
            return carry

        lax.fori_loop(0, T // 128, chunk, 0)
        start(conv_out_copies(s))
        cbm[s, :, conv_lanes] = fsend[s, rows_of(tp), :]

    project(0)
    start(halos(0))

    def project_and_convolve(s, carry):
        project(s)
        start(halos(s))
        convolve(s - 1)
        return carry

    lax.fori_loop(1, SEQS, project_and_convolve, 0)
    arrived(out_1)
    start(out_2)
    start(pair_1)
    convolve(SEQS - 1)

    head_lane = lax.broadcasted_iota(jnp.int32, (1, 256), 1)
    sink_row = jnp.where(head_lane < 128, sink[0], sink[1])

    def widen(s, first):
        kv = kvpad[s, pl.ds(first, WINDOW), :].astype(F32)
        kpad[s, pl.ds(first, WINDOW), :] = jnp.where(low_head, kv, pltpu.roll(kv, 64, 1)).astype(BF16)

    def attend(s, carry):
        arriving = halos(s)
        arriving[2].wait_recv()
        arriving[3].wait_recv()
        widen(s, 0)
        widen(s, WINDOW + T)

        def block(b, carry):
            r = pl.multiple_of(b * 128, 128)
            keys = kpad[s, pl.ds(r, 384), :]
            scores = dot(keys, qz[s, b].reshape(256, 128), ((1,), (1,)))
            off_left = jnp.where((sp == 0) & (b == 0), MASK_VALUE, 0.0)
            off_right = jnp.where((sp == NSP - 1) & (b == T // 128 - 1), MASK_VALUE, 0.0)
            s_0 = scores[:128] + (bias[0] + off_left)
            s_1 = scores[128:256]
            s_2 = scores[256:] + (bias[1] + off_right)
            top = jnp.max(jnp.maximum(jnp.maximum(s_0, s_1), s_2), axis=0, keepdims=True)
            top = jnp.maximum(top, sink_row)
            e_0, e_1, e_2 = jnp.exp(s_0 - top), jnp.exp(s_1 - top), jnp.exp(s_2 - top)
            total = jnp.sum(e_0 + e_1 + e_2, axis=0, keepdims=True) + jnp.exp(sink_row - top)
            logs = top + jnp.log(total)
            log_total[s, :, pl.ds(r, 128)] = jnp.concatenate([logs[:, :128], logs[:, 128:]], axis=0)
            weights = jnp.concatenate([e_0.astype(BF16), e_1.astype(BF16), e_2.astype(BF16)], axis=0)
            out = dot(kvpad[s, pl.ds(r, 384), :], weights, ((0,), (0,)))
            out = out[64:] * (1.0 / total)
            both = jnp.concatenate([out[:, :128], out[:, 128:]], axis=0)
            asend[s, pl.ds(r, 128), :] = both.T.astype(BF16)
            return carry

        lax.fori_loop(0, T // 128, block, 0)
        start(attn_out_copies(s))
        bm[s, :, attn_lanes] = asend[s, rows_of(tp), :]
        return carry

    lax.fori_loop(0, SEQS - 1, attend, 0)
    arrived(out_2)
    start(pair_2)
    attend(SEQS - 1, 0)

    arrived(gains)

    def finish(s, carry):
        for cp in conv_out_copies(s):
            cp.wait_recv()

        def group(g, carry):
            at = pl.ds(pl.multiple_of(g * 16, 16), 16)
            v = cbm[s, at, :].astype(F32)
            mean = jnp.sum(v, axis=-1, keepdims=True) * (1.0 / (TP * 128))
            centred = v - mean
            var = jnp.sum(centred * centred, axis=-1, keepdims=True) * (1.0 / (TP * 128))
            scale = lax.rsqrt(var + EPSILON)
            for n in range(TP):
                u = centred[:, n * 128 : (n + 1) * 128] * scale * gain_all[n, 0:1, :]
                bm[s, at, n * 256 : n * 256 + 128] = jax.nn.silu(u).astype(BF16)
            return carry

        return lax.fori_loop(0, 128 // 16, group, carry, unroll=2)

    lax.fori_loop(0, SEQS, finish, 0)
    for s in range(SEQS):
        for cp in attn_out_copies(s):
            cp.wait_recv()
    arrived(pair_1)
    arrived(pair_2)

    def out_project(p, carry):
        zz, xx = p // (X // 2), (p % (X // 2)) * 2
        pieces = [
            jnp.concatenate([o_w[cc, hh, zz, xx], o_w[cc, hh, zz, xx + 1]], axis=1)
            for cc in range(CORES)
            for hh in range(2)
        ]
        acc = dot(bm[...].reshape(SEQS * 128, TP * 256), jnp.concatenate(pieces, axis=0))
        columns = pl.ds(pl.multiple_of(p * 256, 256), 256)
        mixed[:, :, columns] = acc.astype(BF16).reshape(SEQS, 128, 256)
        return carry

    lax.fori_loop(0, NSP // 2, out_project, 0)

    for cp in in_1 + in_2 + out_0 + gains + out_1 + out_2 + pair_1 + pair_2:
        cp.wait_send()

    def drain(s, carry):
        for cp in halos(s) + conv_out_copies(s) + attn_out_copies(s):
            cp.wait_send()
        return carry

    lax.fori_loop(0, SEQS, drain, 0)


def on_device(
    grid_shape,
    tokens,
    norm_gain,
    conv_value_weight,
    conv_gate_weight,
    query_weight,
    key_weight,
    value_weight,
    conv_taps,
    conv_gain,
    sink_logit,
    out_conv_weight,
    out_attn_weight,
):
    seqs, toks, width = tokens.shape
    xs, zs, ys, tps = grid_shape
    offset = lax.axis_index("sp") * toks
    positions = (offset + jnp.arange(toks, dtype=jnp.int32)).astype(F32)
    lanes = jnp.arange(128)
    half = HEAD_DIM // 2
    inverse = ROPE_BASE ** (-(lanes % half).astype(F32) / half)
    angles = positions[:, None] * inverse[None, :]
    cosine = jnp.cos(angles)
    sine = jnp.sin(angles) * jnp.where(lanes % HEAD_DIM < half, -1.0, 1.0)[None, :]

    n_copies = 4 * (xs - 1) + 4 * (zs - 1) + (ys - 1) + (tps - 1) + 2
    n_copies += (xs - 1) + (zs - 1) + 4 * seqs + 2 * (tps - 1) * seqs
    vmem = pl.BlockSpec(memory_space=pltpu.VMEM)
    call = pl.pallas_call(
        functools.partial(kernel, (seqs, toks, width, xs, zs, ys, tps)),
        out_shape=(
            jax.ShapeDtypeStruct((seqs, toks // tps, width), BF16),
            jax.ShapeDtypeStruct((seqs, 2, toks), F32),
        ),
        in_specs=[pl.BlockSpec(memory_space=pl.ANY)]
        + [vmem] * 8
        + [pl.BlockSpec(memory_space=pltpu.SMEM)]
        + [vmem] * 4,
        out_specs=(vmem, vmem),
        scratch_shapes=[
            pltpu.VMEM((3, LN_ROWS, width), BF16),
            pltpu.VMEM((16, width), F32),
            pltpu.VMEM((seqs * toks, width), BF16),
            pltpu.VMEM((zs, xs, 128, 256), BF16),
            pltpu.VMEM((zs, xs, 128, 256), BF16),
            pltpu.VMEM((CORES, 2, zs, xs, ys // 2 * 256, 128), BF16),
            pltpu.VMEM((tps, 8, 128), F32),
            pltpu.VMEM((31, 128), F32),
            pltpu.VMEM((seqs, toks + 2 * RIM, 128), F32),
            pltpu.VMEM((seqs, toks // 128, 2, 128, 128), BF16),
            pltpu.VMEM((seqs, toks + 2 * WINDOW, 128), BF16),
            pltpu.VMEM((seqs, toks + 2 * WINDOW, 128), BF16),
            pltpu.VMEM((2, WINDOW, 256), F32),
            pltpu.VMEM((seqs, toks, 128), BF16),
            pltpu.VMEM((seqs, toks, 128), BF16),
            pltpu.VMEM((seqs, toks // tps, tps * 128), BF16),
            pltpu.VMEM((seqs, toks // tps, tps * 256), BF16),
            pltpu.SemaphoreType.DMA((3,)),
            pltpu.SemaphoreType.DMA((n_copies,)),
            pltpu.SemaphoreType.DMA((n_copies,)),
        ],
        compiler_params=pltpu.CompilerParams(
            collective_id=0, has_side_effects=True, vmem_limit_bytes=63 * 2**20
        ),
        name="layer",
    )
    return call(
        tokens,
        norm_gain.reshape(1, -1),
        conv_value_weight,
        conv_gate_weight,
        query_weight,
        key_weight,
        value_weight,
        conv_taps,
        conv_gain.reshape(1, -1),
        sink_logit,
        out_conv_weight,
        out_attn_weight,
        cosine,
        sine,
    )


def solution(mesh):
    placed = (
        P(None, "sp", None),
        P(),
        P("sp", "tp"),
        P("sp", "tp"),
        P("sp", "tp"),
        P("sp", "tp"),
        P("sp", "tp"),
        P(None, "tp"),
        P("tp"),
        P("tp"),
        P("tp", "sp"),
        P("tp", "sp"),
    )
    xs = int(round(mesh.shape["sp"] ** 0.5))
    shape = (xs, mesh.shape["sp"] // xs, mesh.shape["tp"] // CORES, mesh.shape["tp"])
    return jax.shard_map(
        functools.partial(on_device, shape),
        mesh=mesh,
        in_specs=placed,
        out_specs=(P(None, ("sp", "tp"), None), P(None, "tp", "sp")),
        check_vma=False,
    )
```

profile of v0, /device:TPU:1, one launch (start us, length us, event | category | flops | bytes accessed | tf_op | source)
XLA Modules:
  0.0 102.0 jit_solution(16638735900225717664)
XLA Ops:
  0.7 1.3 %reshape.39.norm_gain = bf16[1,2048]{1,0:T(2,128)(2,1)} reshape(bf16[2048]{0:T(1024)(128)(2,1)} %param.13) | data formatting | bytes 8192 | tf_op jit(solution)/shard_map/reshape | solution.py:507
  1.9 1.4 %copy.14.w_key = bf16[128,64]{1,0:T(8,128)(2,1)} copy(bf16[128,64]{0,1:T(8,128)(2,1)} %param.17) | data formatting | bytes 32768 | tf_op args[5]
  3.4 1.4 %copy.15.w_val = bf16[128,64]{1,0:T(8,128)(2,1)} copy(bf16[128,64]{0,1:T(8,128)(2,1)} %param.18) | data formatting | bytes 32768 | tf_op args[6]
  4.8 3.0 %fusion = (f32[1024,128]{1,0:T(8,128)}, f32[1024,128]{1,0:T(8,128)}) fusion(f32[128]{0:T(128)S(1)} %get-tuple-element.4, f32[128]{0:T(128)S(1)} %get-tuple-element.5, f32[1024]{0:T(1024)S(1)} %add_convert_fusion), kind=kLoop, calls=%fused_computation.2 | loop fusion | flops 262144 | bytes 1053696 | tf_op jit(solution)/shard_map/mul | solution.py:462
  7.8 90.3 %layer.1 = (bf16[4,128,2048]{2,1,0:T(8,128)(2,1)}, f32[4,2,1024]{2,1,0:T(2,128)}) custom-call(bf16[4,1024,2048]{2,1,0:T(8,128)(2,1)} %tokens.1, bf16[1,2048]{1,0:T(2,128)(2,1)} %reshape.39.norm_gain, bf16[128,128]{1,0:T(8,128)(2,1)} %w_value.1, bf16[128,128]{1,0:T(8,128)(2,1)} %w_gate.1, bf16[128,128]{1,0:T(8,128)(2,1)} %w_query.1, ...), custom_call_target="tpu_custom_call" | custom-call | tf_op jit(solution)/shard_map/layer/pallas_call | solution.py:505
  98.2 0.0 copy-start
  98.2 3.2 %copy.18 = bf16[4,128,2048]{2,1,0:T(8,128)(2,1)} copy(bf16[4,128,2048]{2,1,0:T(8,128)(2,1)} %get-tuple-element.8) | data formatting | bytes 4194304
  101.3 0.0 copy-done
  101.3 0.6 copy.19
  (2 shorter events, 0.0 us)
Async XLA Ops:
  98.2 3.2 %copy-start = (f32[4,2,1024]{2,1,0:T(2,128)S(1)}, f32[4,2,1024]{2,1,0:T(2,128)}, u32[]{:S(2)}) copy-start(f32[4,2,1024]{2,1,0:T(2,128)} %get-tuple-element.9) | copy-start | bytes 98308
where the time goes:
time: 103 us; the launch traced here: 102 us
  Pallas kernels  90.3 us (88%)
  local copies, waits for them, and re-layouts  7.92 us (8%)
  other arithmetic  3.06 us (3%)
    pallas_call x1, Pallas kernels, on_device(): call(tokens, norm_gain.reshape(1, -1), conv_value_weight, conv_gate_weigh...  90.3 us
    unnamed x6, local copies, waits for them, and re-layouts  6.63 us
    mul x1, other arithmetic, on_device(): jnp.sin(angles) * jnp.where(lanes % HEAD_DIM < half, -1.0, 1.0)[None, :]  3.04 us

commit v1 on v0

v1 whole, which is shorter than its diff:
```python
import functools

import jax
import jax.numpy as jnp
import numpy as np
from jax import lax
from jax.experimental import pallas as pl
from jax.experimental.pallas import tpu as pltpu
from jax.sharding import PartitionSpec as P

MESH = pl.DeviceIdType.MESH
F32 = jnp.float32
BF16 = jnp.bfloat16

HEAD_DIM = 64
WINDOW = 128
EPSILON = 1e-06
ROPE_BASE = 10000.0
MASK_VALUE = -1e30
RIM = 16
LN_ROWS = 256
CORES = 2
SLOTS = 6


def dot(a, b, dims=((1,), (0,))):
    return lax.dot_general(a, b, (dims, ((), ())), preferred_element_type=F32)


def kernel(
    dims,
    tokens,
    norm_gain,
    w_value,
    w_gate,
    w_query,
    w_key,
    w_val,
    conv_taps,
    conv_gain,
    sink,
    w_oc,
    w_oa,
    turns,
    mixed,
    log_total,
    tbuf,
    gain_buf,
    normed,
    w_a,
    w_b,
    o_w,
    gain_all,
    taps_buf,
    key_buf,
    gain_rows,
    taps_rows,
    conv_gain_row,
    turn_buf,
    cos_ref,
    sin_ref,
    gpad,
    qz,
    kpad,
    val_t,
    edges,
    bias,
    fsend,
    asend,
    cbm,
    bm,
    tok_sem,
    load_sem,
    send_sem,
    recv_sem,
):
    SEQS, T, D, X, Z, Y, TP = dims
    NSP = X * Z
    per_seq = T // LN_ROWS
    n_blocks = SEQS * per_seq
    sp, tp = lax.axis_index("sp"), lax.axis_index("tp")
    z, x = sp // X, sp % X
    y, c = tp // CORES, tp % CORES
    half_y = Y // 2
    yh, yl = y // half_y, y % half_y
    slot = c * Y + y

    def at_x(d):
        return (z * X + (x + d) % X, tp)

    def at_z(d):
        return (((z + d) % Z) * X + x, tp)

    def at_y(d):
        return (sp, ((y + d) % Y) * CORES + c)

    def at_tp(d):
        return (sp, (tp + d) % TP)

    partner = (sp, y * CORES + (1 - c))
    right = ((sp + 1) % NSP, tp)
    left = ((sp + NSP - 1) % NSP, tp)

    counter = [0]

    def ids(n):
        first = counter[0]
        counter[0] += n
        return first

    def remote(src, dst, i, device):
        return pltpu.make_async_remote_copy(
            src_ref=src,
            dst_ref=dst,
            send_sem=send_sem.at[i],
            recv_sem=recv_sem.at[i],
            device_id=device,
            device_id_type=MESH,
        )

    def start(copies):
        for cp in copies:
            cp.start()

    def group_of(i, pairs, whole):
        copies = [remote(src, dst, i, device) for src, dst, device in pairs]
        return copies, remote(whole, whole, i, right)

    def arrived(group):
        group[1].wait_recv()

    def left_here(group):
        group[1].wait_send()

    class Ring:
        def __init__(self, part, me, size, at):
            i = ids(6)
            ahead, behind = at(1), at(size - 1)
            lo, hi = part(me, 0), part(me, 1)
            self.direct = [remote(lo, lo, i, ahead)]
            self.relayed, self.late = [], [remote(hi, hi, i + 1, ahead)]
            if size == 2:
                return
            self.direct.append(remote(hi, hi, i + 2, behind))
            self.late.append(remote(lo, lo, i + 3, behind))
            near, far = part((me + size - 1) % size, 0), part((me + 1) % size, 1)
            self.passed = [near, far]
            self.rest = [part((me + size - 1) % size, 1), part((me + 1) % size, 0)]
            self.relayed = [remote(near, near, i + 4, ahead), remote(far, far, i + 5, behind)]

        def begin(self):
            start(self.direct)
            start(self.late)

        def relay(self):
            for cp in self.direct:
                cp.wait_recv()
            start(self.relayed)

        def finish(self):
            for cp in self.late + self.relayed:
                cp.wait_recv()

        def drain(self):
            for cp in self.direct + self.late + self.relayed:
                cp.wait_send()

    def tok_copy(i):
        seq, r = i // per_seq, (i % per_seq) * LN_ROWS
        return pltpu.make_async_copy(
            tokens.at[seq, pl.ds(pl.multiple_of(r, LN_ROWS), LN_ROWS)],
            tbuf.at[i % SLOTS],
            tok_sem.at[i % SLOTS],
        )

    barrier = pltpu.get_barrier_semaphore()
    greeted = (
        [at_x(d) for d in range(1, X)]
        + [at_z(d) for d in range(1, Z)]
        + [left, right]
        + [at_tp(d) for d in range(1, TP)]
    )
    for device in greeted:
        pl.semaphore_signal(barrier, inc=1, device_id=device, device_id_type=MESH)

    tile_at = pl.multiple_of(yl * 256, 256)
    wanted = [
        (w_value, w_a.at[z, x, :, pl.ds(0, 128)]),
        (w_gate, w_a.at[z, x, :, pl.ds(128, 128)]),
        (w_query, w_b.at[z, x, :, pl.ds(0, 128)]),
        (w_oc, o_w.at[c, yh, z, x, pl.ds(tile_at, 128)]),
        (w_oa, o_w.at[c, yh, z, x, pl.ds(tile_at + 128, 128)]),
        (w_key, key_buf.at[pl.ds(0, 64)]),
        (w_val, key_buf.at[pl.ds(64, 64)]),
        (conv_taps, taps_rows),
        (turns.at[0], turn_buf.at[0]),
        (turns.at[1], turn_buf.at[1]),
        (norm_gain, gain_rows),
        (conv_gain, conv_gain_row),
    ]
    loads = [pltpu.make_async_copy(a, b, load_sem.at[n]) for n, (a, b) in enumerate(wanted)]
    for n in (5, 6, 8, 9, 0, 1, 2, 3, 4, 7, 10, 11):
        loads[n].start()

    for n in range(SLOTS - 1):
        tok_copy(n).start()
    for n in (8, 9, 10):
        loads[n].wait()
    run = turn_buf.shape[1] - NSP - 32
    cos_s, sin_s = turn_buf[0, pl.ds(run + 32 + sp, 1), :], turn_buf[1, pl.ds(run + 32 + sp, 1), :]
    cos_b, sin_b = turn_buf[0, run : run + 32, :], turn_buf[1, run : run + 32, :]
    cos_bs, sin_bs = cos_b * cos_s - sin_b * sin_s, sin_b * cos_s + cos_b * sin_s
    low_half = (lax.broadcasted_iota(jnp.int32, (1, 128), 1) % HEAD_DIM) < HEAD_DIM // 2
    sign = jnp.where(low_half, -1.0, 1.0)

    def turn(n, carry):
        cos_a, sin_a = turn_buf[0, pl.ds(n, 1), :], turn_buf[1, pl.ds(n, 1), :]
        at = pl.ds(pl.multiple_of(n * 32, 32), 32)
        cos_ref[at, :] = cos_bs * cos_a - sin_bs * sin_a
        sin_ref[at, :] = (sin_bs * cos_a + cos_bs * sin_a) * sign
        return carry

    lax.fori_loop(0, T // 32, turn, 0, unroll=2)

    for n in (5, 6, 7):
        loads[n].wait()
    w_b[z, x, :, 128:256] = key_buf[...].astype(F32).T.astype(BF16)
    taps_buf[...] = taps_rows[...].astype(F32)
    for n in range(D // 128):
        gain_buf[:, n * 128 : (n + 1) * 128] = jnp.broadcast_to(
            gain_rows[n : n + 1, :].astype(F32), (16, 128)
        )
    loads[11].wait()
    gain_all[slot] = jnp.broadcast_to(conv_gain_row[...].astype(F32), (8, 128))
    key_i = lax.broadcasted_iota(jnp.int32, (WINDOW, 256), 0)
    query_i = lax.broadcasted_iota(jnp.int32, (WINDOW, 256), 1) % WINDOW
    bias[0] = jnp.where(key_i >= query_i, 0.0, MASK_VALUE)
    bias[1] = jnp.where(key_i <= query_i, 0.0, MASK_VALUE)

    half_x, half_z = X // 2, Z // 2
    in_1 = [
        group_of(ids(1), [(w_a.at[z, x], w_a.at[z, x], at_x(d)) for d in range(1, X)], w_a.at[0, pl.ds(0, X - 1)]),
        group_of(ids(1), [(w_b.at[z, x], w_b.at[z, x], at_z(d)) for d in range(1, Z)], w_b.at[pl.ds(0, Z - 1), 0]),
    ]
    in_2 = [
        Ring(lambda k, h: w_a.at[k, pl.ds(h * half_x, half_x)], z, Z, at_z),
        Ring(lambda k, h: w_b.at[pl.ds(h * half_z, half_z), k], x, X, at_x),
    ]
    tile = o_w.at[c, yh, z, x, pl.ds(tile_at, 256)]
    out_0 = group_of(ids(1), [(tile, tile, at_y(d)) for d in range(1, Y)], fsend.at[0, pl.ds(0, (Y - 1) * 256)])
    own_gain = gain_all.at[slot]
    gains = group_of(ids(1), [(own_gain, own_gain, at_tp(d)) for d in range(1, TP)], gain_all.at[pl.ds(0, TP - 1)])
    out_1 = [
        group_of(
            ids(1),
            [(o_w.at[c, 0, z, x], o_w.at[c, 0, z, x], at_x(d)) for d in range(1, X)],
            o_w.at[0, 0, 0, pl.ds(0, X - 1)],
        ),
        group_of(
            ids(1),
            [(o_w.at[c, 1, z, x], o_w.at[c, 1, z, x], at_z(d)) for d in range(1, Z)],
            o_w.at[0, 0, pl.ds(0, Z - 1), 0],
        ),
    ]
    out_2 = [
        Ring(lambda k, h: o_w.at[c, 0, k, pl.ds(h * half_x, half_x)], z, Z, at_z),
        Ring(lambda k, h: o_w.at[c, 1, pl.ds(h * half_z, half_z), k], x, X, at_x),
    ]

    def to_partner(d):
        row, column = o_w.at[c, 0, (z + d) % Z], o_w.at[c, 1, :, (x + d) % X]
        return [(row, row, partner), (column, column, partner)]

    pair_1 = group_of(ids(1), to_partner(0), o_w.at[0, 0, pl.ds(0, 2)])
    if X == 2:
        early, late = [], to_partner(1)
        late_whole = o_w.at[0, 0, pl.ds(0, 2)]
    else:
        passed = [ref for ring in out_2 for ref in ring.passed]
        early = [(ref, ref, partner) for ref in passed]
        rest = [ref for ring in out_2 for ref in ring.rest]
        late = [(ref, ref, partner) for ref in rest] + to_partner(2)
        late_whole = o_w.at[0, 0]
    pair_2 = group_of(ids(1), early, o_w.at[0, 0, pl.ds(0, 2)])
    pair_3 = group_of(ids(1), late, late_whole)

    rim_i, keys_i = ids(SEQS), ids(SEQS)

    def rims(s):
        return group_of(
            rim_i + s,
            [
                (gpad.at[s, pl.ds(RIM, RIM)], gpad.at[s, pl.ds(RIM + T, RIM)], left),
                (gpad.at[s, pl.ds(T, RIM)], gpad.at[s, pl.ds(0, RIM)], right),
            ],
            gpad.at[0, pl.ds(0, 2 * RIM)],
        )

    def edge_keys(s):
        return group_of(
            keys_i + s,
            [(edges.at[s, 1], edges.at[s, 3], left), (edges.at[s, 2], edges.at[s, 0], right)],
            edges.at[0, pl.ds(0, 2)],
        )

    conv_i, attn_i = ids(SEQS), ids(SEQS)
    peers_rows = fsend.at[0, pl.ds(0, (TP - 1) * 128)]

    def rows_of(device_tp):
        return pl.ds(pl.multiple_of(device_tp * 128, 128), 128)

    conv_lanes = pl.ds(pl.multiple_of(slot * 128, 128), 128)
    attn_lanes = pl.ds(pl.multiple_of(slot * 256 + 128, 128), 128)

    def conv_out_copies(s):
        return group_of(
            conv_i + s,
            [
                (fsend.at[s, rows_of((tp + d) % TP)], cbm.at[s, :, conv_lanes], at_tp(d))
                for d in range(1, TP)
            ],
            peers_rows,
        )

    def attn_out_copies(s):
        return group_of(
            attn_i + s,
            [
                (asend.at[s, rows_of((tp + d) % TP)], bm.at[s, :, attn_lanes], at_tp(d))
                for d in range(1, TP)
            ],
            peers_rows,
        )

    for n in range(5):
        loads[n].wait()
    with jax.named_scope("greet"):
        pl.semaphore_wait(barrier, len(greeted))
    for group in in_1:
        start(group[0])
    start(out_0[0])
    start(gains[0])

    def ln_block(i, carry):
        tok_copy(i).wait()

        @pl.when(i + SLOTS - 1 < n_blocks)
        def _():
            tok_copy(i + SLOTS - 1).start()

        def group(g, carry):
            at = pl.ds(pl.multiple_of(i * LN_ROWS, LN_ROWS) + pl.multiple_of(g * 16, 16), 16)
            v = tbuf[i % SLOTS, pl.ds(pl.multiple_of(g * 16, 16), 16), :].astype(F32)
            mean = jnp.sum(v, axis=-1, keepdims=True) * (1.0 / D)
            centred = v - mean
            var = jnp.sum(centred * centred, axis=-1, keepdims=True) * (1.0 / D)
            out = centred * lax.rsqrt(var + EPSILON) * gain_buf[...]
            normed[at, :] = out.astype(BF16)
            return carry

        return lax.fori_loop(0, LN_ROWS // 16, group, carry, unroll=16)

    cuts = (0, n_blocks * 3 // 8, n_blocks * 7 // 8, n_blocks)
    with jax.named_scope("norm_a"):
        lax.fori_loop(cuts[0], cuts[1], ln_block, 0)
    with jax.named_scope("wait_in_1"):
        for group in in_1:
            arrived(group)
    for ring in in_2:
        ring.begin()
    with jax.named_scope("norm_b"):
        lax.fori_loop(cuts[1], cuts[2], ln_block, 0)
    with jax.named_scope("wait_relay"):
        for ring in in_2:
            ring.relay()
    with jax.named_scope("wait_out_0"):
        arrived(out_0)
    for group in out_1:
        start(group[0])
    with jax.named_scope("norm_c"):
        lax.fori_loop(cuts[2], cuts[3], ln_block, 0)
    with jax.named_scope("wait_in_2"):
        for ring in in_2:
            ring.finish()

    lane = lax.broadcasted_iota(jnp.int32, (1, 128), 1)
    low_head = lane < HEAD_DIM

    def swapped(v):
        return jnp.where(low_half, pltpu.roll(v, 96, 1), pltpu.roll(v, 32, 1))

    def project(s, starts):
        n = 256 // len(starts)
        at = [pl.ds(pl.multiple_of(s * T + r, 128), n) for r in starts]
        rows = jnp.concatenate([normed[rs, :] for rs in at], axis=0)
        a = dot(rows, w_a[...].reshape(D, 256))
        gated = a[:, :128] * jax.nn.sigmoid(a[:, 128:])
        gated = gated.astype(BF16).astype(F32)
        b = dot(rows, w_b[...].reshape(D, 256))
        at = [pl.ds(pl.multiple_of(r, 128), n) for r in starts]
        cosine = jnp.concatenate([cos_ref[rs, :] for rs in at], axis=0)
        sine = jnp.concatenate([sin_ref[rs, :] for rs in at], axis=0)
        q, kv = b[:, :128], b[:, 128:]
        q = (q * cosine + swapped(q) * sine) * (HEAD_DIM**-0.5)
        zero = jnp.zeros_like(q)
        q_0 = jnp.where(low_head, q, zero).astype(BF16)
        q_1 = jnp.where(low_head, zero, q).astype(BF16)
        turned = kv * cosine + swapped(kv) * sine
        twice = jnp.where(low_head, turned, pltpu.roll(turned, 64, 1)).astype(BF16)
        kv = jnp.where(low_head, turned, kv).astype(BF16)
        for k in range(2):
            r = pl.multiple_of(starts[k] if len(starts) == 2 else starts[0] + k * 128, 128)
            part = slice(k * 128, (k + 1) * 128)
            gpad[s, pl.ds(RIM + r, 128), :] = gated[part]
            qz[s, r // 128, 0] = q_0[part]
            qz[s, r // 128, 1] = q_1[part]
            kpad[s, pl.ds(WINDOW + r, 128), :] = twice[part]
            val_t[s, :, pl.ds(WINDOW + r, 128)] = kv[part].T[64:]
            if len(starts) == 2:
                edges[s, k + 1] = kv[part]

    def convolve(s):
        with jax.named_scope("wait_rim"):
            arrived(rims(s))

        @pl.when(sp == 0)
        def _():
            gpad[s, pl.ds(0, RIM), :] = jnp.zeros((RIM, 128), F32)

        @pl.when(sp == NSP - 1)
        def _():
            gpad[s, pl.ds(RIM + T, RIM), :] = jnp.zeros((RIM, 128), F32)

        def chunk(k, carry):
            r = pl.multiple_of(k * 128, 128)
            total = jnp.zeros((128, 128), F32)
            for j in range(31):
                total = total + gpad[s, pl.ds(r + (j + 1), 128), :] * taps_buf[pl.ds(j, 1), :]
            fsend[s, pl.ds(r, 128), :] = total.astype(BF16)
            return carry

        with jax.named_scope("conv"):
            lax.fori_loop(0, T // 128, chunk, 0)
        start(conv_out_copies(s)[0])
        cbm[s, :, conv_lanes] = fsend[s, rows_of(tp), :]

    def project_edges(s, carry):
        project(s, (0, T - 128))
        return carry

    def send_edges(s, carry):
        start(edge_keys(s)[0])
        start(rims(s)[0])
        return carry

    def project_inner(k, carry):
        inner = T // 256 - 1
        project(k // inner, (128 + (k % inner) * 256,))
        return carry

    n_inner = SEQS * (T // 256 - 1)
    inner_cut = n_inner // 2
    with jax.named_scope("project_edges"):
        lax.fori_loop(0, SEQS, project_edges, 0, unroll=2)
    lax.fori_loop(0, SEQS, send_edges, 0)
    with jax.named_scope("project_a"):
        lax.fori_loop(0, inner_cut, project_inner, 0, unroll=3)
    with jax.named_scope("wait_out_1"):
        for group in out_1:
            arrived(group)
    with jax.named_scope("wait_rims"):
        for ring in out_2:
            ring.begin()
    start(pair_1[0])
    with jax.named_scope("project_b"):
        lax.fori_loop(inner_cut, n_inner, project_inner, 0, unroll=3)

    def each_convolve(s, carry):
        convolve(s)
        return carry

    lax.fori_loop(0, SEQS, each_convolve, 0)
    with jax.named_scope("wait_out_relay"):
        for ring in out_2:
            ring.relay()
    start(pair_2[0])

    head_lane = lax.broadcasted_iota(jnp.int32, (1, 256), 1)
    sink_row = jnp.where(head_lane < 128, sink[0], sink[1])

    def widen(s, e, first):
        kv = edges[s, e].astype(F32)
        kpad[s, pl.ds(first, WINDOW), :] = jnp.where(low_head, kv, pltpu.roll(kv, 64, 1)).astype(BF16)
        val_t[s, :, pl.ds(first, WINDOW)] = edges[s, e].T[64:]

    def attend(s, carry):
        @pl.when(s == SEQS - 1)
        def _():
            with jax.named_scope("wait_out_2"):
                for ring in out_2:
                    ring.finish()
            start(pair_3[0])

        with jax.named_scope("wait_keys"):
            arrived(edge_keys(s))
        widen(s, 0, 0)
        widen(s, 3, WINDOW + T)

        def block(b, carry):
            r = pl.multiple_of(b * 128, 128)
            keys = kpad[s, pl.ds(r, 384), :]
            scores = dot(keys, qz[s, b].reshape(256, 128), ((1,), (1,)))
            off_left = jnp.where((sp == 0) & (b == 0), MASK_VALUE, 0.0)
            off_right = jnp.where((sp == NSP - 1) & (b == T // 128 - 1), MASK_VALUE, 0.0)
            s_0 = scores[:128] + (bias[0] + off_left)
            s_1 = scores[128:256]
            s_2 = scores[256:] + (bias[1] + off_right)
            top = jnp.max(jnp.maximum(jnp.maximum(s_0, s_1), s_2), axis=0, keepdims=True)
            top = jnp.maximum(top, sink_row)
            e_0, e_1, e_2 = jnp.exp(s_0 - top), jnp.exp(s_1 - top), jnp.exp(s_2 - top)
            total = jnp.sum(e_0 + e_1 + e_2, axis=0, keepdims=True) + jnp.exp(sink_row - top)
            logs = top + jnp.log(total)
            log_total[s, :, pl.ds(r, 128)] = jnp.concatenate([logs[:, :128], logs[:, 128:]], axis=0)
            weights = jnp.concatenate([e_0.astype(BF16), e_1.astype(BF16), e_2.astype(BF16)], axis=0)
            out = dot(val_t[s, :, pl.ds(r, 384)], weights) * (1.0 / total)
            both = jnp.concatenate([out[:, :128], out[:, 128:]], axis=0)
            asend[s, pl.ds(r, 128), :] = both.astype(BF16).T
            return carry

        with jax.named_scope("attend"):
            lax.fori_loop(0, T // 128, block, 0, unroll=min(8, T // 128))
        start(attn_out_copies(s)[0])
        bm[s, :, attn_lanes] = asend[s, rows_of(tp), :]
        return carry

    lax.fori_loop(0, SEQS, attend, 0)

    arrived(gains)

    def finish(s):
        with jax.named_scope("wait_conv"):
            arrived(conv_out_copies(s))

        def group(g, carry):
            at = pl.ds(pl.multiple_of(g * 16, 16), 16)
            v = cbm[s, at, :].astype(F32)
            mean = jnp.sum(v, axis=-1, keepdims=True) * (1.0 / (TP * 128))
            centred = v - mean
            var = jnp.sum(centred * centred, axis=-1, keepdims=True) * (1.0 / (TP * 128))
            scale = lax.rsqrt(var + EPSILON)
            for n in range(TP):
                u = centred[:, n * 128 : (n + 1) * 128] * scale * gain_all[n, 0:1, :]
                bm[s, at, n * 256 : n * 256 + 128] = jax.nn.silu(u).astype(BF16)
            return carry

        with jax.named_scope("channel_norm"):
            lax.fori_loop(0, 128 // 16, group, 0, unroll=8)

    def out_rows(s, carry):
        finish(2 * s)
        finish(2 * s + 1)
        with jax.named_scope("wait_attn"):
            arrived(attn_out_copies(2 * s))
            arrived(attn_out_copies(2 * s + 1))

        @pl.when(s == 0)
        def _():
            with jax.named_scope("wait_pair"):
                arrived(pair_1)
                if X > 2:
                    arrived(pair_2)
                arrived(pair_3)

        def out_project(p, carry):
            zz, xx = p // (X // 2), (p % (X // 2)) * 2
            pieces = [
                jnp.concatenate([o_w[cc, hh, zz, xx], o_w[cc, hh, zz, xx + 1]], axis=1)
                for cc in range(CORES)
                for hh in range(2)
            ]
            rows = bm[pl.ds(2 * s, 2)].reshape(256, TP * 256)
            acc = dot(rows, jnp.concatenate(pieces, axis=0))
            columns = pl.ds(pl.multiple_of(p * 256, 256), 256)
            mixed[pl.ds(2 * s, 2), :, columns] = acc.astype(BF16).reshape(2, 128, 256)
            return carry

        with jax.named_scope("out_project"):
            lax.fori_loop(0, NSP // 2, out_project, 0, unroll=2)
        return carry

    lax.fori_loop(0, SEQS // 2, out_rows, 0)

    for group in in_1 + [out_0, gains] + out_1 + [pair_1, pair_3] + ([pair_2] if X > 2 else []):
        left_here(group)
    for ring in in_2 + out_2:
        ring.drain()

    def drain(s, carry):
        for group in (rims(s), edge_keys(s), conv_out_copies(s), attn_out_copies(s)):
            left_here(group)
        return carry

    lax.fori_loop(0, SEQS, drain, 0)


def on_device(
    grid_shape,
    tokens,
    norm_gain,
    conv_value_weight,
    conv_gate_weight,
    query_weight,
    key_weight,
    value_weight,
    conv_taps,
    conv_gain,
    sink_logit,
    out_conv_weight,
    out_attn_weight,
):
    seqs, toks, width = tokens.shape
    xs, zs, ys, tps = grid_shape
    n_sp = xs * zs
    half = HEAD_DIM // 2
    inverse = (ROPE_BASE ** (-np.arange(half, dtype=np.float32) / half)).astype(np.float32)
    parts = [np.arange(toks // 32) * 32, np.arange(32), np.arange(n_sp) * toks]
    angles = np.concatenate(parts)[:, None] * np.tile(inverse.astype(np.float64), 4)[None, :]
    turns = np.stack([np.cos(angles), np.sin(angles)]).astype(np.float32)

    n_copies = 2 + 12 + 2 + 2 + 12 + 3 + 4 * seqs
    vmem = pl.BlockSpec(memory_space=pltpu.VMEM)
    far = pl.BlockSpec(memory_space=pl.ANY)
    call = pl.pallas_call(
        functools.partial(kernel, (seqs, toks, width, xs, zs, ys, tps)),
        out_shape=(
            pltpu.VMEM((seqs, toks // tps, width), BF16),
            pltpu.VMEM((seqs, 2, toks), F32),
        ),
        in_specs=[far] * 9 + [pl.BlockSpec(memory_space=pltpu.SMEM)] + [far] * 3,
        out_specs=(vmem, vmem),
        scratch_shapes=[
            pltpu.VMEM((SLOTS, LN_ROWS, width), BF16),
            pltpu.VMEM((16, width), F32),
            pltpu.VMEM((seqs * toks, width), BF16),
            pltpu.VMEM((zs, xs, 128, 256), BF16),
            pltpu.VMEM((zs, xs, 128, 256), BF16),
            pltpu.VMEM((CORES, 2, zs, xs, ys // 2 * 256, 128), BF16),
            pltpu.VMEM((tps, 8, 128), F32),
            pltpu.VMEM((31, 128), F32),
            pltpu.VMEM((128, 128), BF16),
            pltpu.VMEM((width // 128, 128), BF16),
            pltpu.VMEM((31, 128), BF16),
            pltpu.VMEM((1, 128), BF16),
            pltpu.VMEM(turns.shape, F32),
            pltpu.VMEM((toks, 128), F32),
            pltpu.VMEM((toks, 128), F32),
            pltpu.VMEM((seqs, toks + 2 * RIM, 128), F32),
            pltpu.VMEM((seqs, toks // 128, 2, 128, 128), BF16),
            pltpu.VMEM((seqs, toks + 2 * WINDOW, 128), BF16),
            pltpu.VMEM((seqs, HEAD_DIM, toks + 2 * WINDOW), BF16),
            pltpu.VMEM((seqs, 4, WINDOW, 128), BF16),
            pltpu.VMEM((2, WINDOW, 256), F32),
            pltpu.VMEM((seqs, toks, 128), BF16),
            pltpu.VMEM((seqs, toks, 128), BF16),
            pltpu.VMEM((seqs, toks // tps, tps * 128), BF16),
            pltpu.VMEM((seqs, toks // tps, tps * 256), BF16),
            pltpu.SemaphoreType.DMA((SLOTS,)),
            pltpu.SemaphoreType.DMA((12,)),
            pltpu.SemaphoreType.DMA((n_copies,)),
            pltpu.SemaphoreType.DMA((n_copies,)),
        ],
        compiler_params=pltpu.CompilerParams(
            collective_id=0, has_side_effects=True, vmem_limit_bytes=54 * 2**20
        ),
        name="layer",
    )
    return call(
        tokens,
        norm_gain.reshape(-1, 128),
        conv_value_weight,
        conv_gate_weight,
        query_weight,
        key_weight.T,
        value_weight.T,
        conv_taps,
        conv_gain.reshape(1, -1),
        sink_logit,
        out_conv_weight,
        out_attn_weight,
        jnp.asarray(turns),
    )


def solution(mesh):
    placed = (
        P(None, "sp", None),
        P(),
        P("sp", "tp"),
        P("sp", "tp"),
        P("sp", "tp"),
        P("sp", "tp"),
        P("sp", "tp"),
        P(None, "tp"),
        P("tp"),
        P("tp"),
        P("tp", "sp"),
        P("tp", "sp"),
    )
    xs = int(round(mesh.shape["sp"] ** 0.5))
    shape = (xs, mesh.shape["sp"] // xs, mesh.shape["tp"] // CORES, mesh.shape["tp"])
    return jax.shard_map(
        functools.partial(on_device, shape),
        mesh=mesh,
        in_specs=placed,
        out_specs=(P(None, ("sp", "tp"), None), P(None, "tp", "sp")),
        check_vma=False,
    )
```

time: 103 us -> 68 us (0.66)
  Pallas kernels: 90.3 us -> 65.3 us
  local copies, waits for them, and re-layouts: 7.92 us -> 1.94 us
  other arithmetic: 3.06 us -> 0 us
    pallas_call x1, Pallas kernels: 90.3 us -> 65.3 us  [on_device(): call(tokens, norm_gain.reshape(-1, 128), conv_value_weight, conv_gate_wei...]
    unnamed x6 -> x2, local copies, waits for them, and re-layouts: 6.63 us -> 1.94 us
    mul x1 -> x0, other arithmetic: 3.04 us -> none  [on_device(): jnp.sin(angles) * jnp.where(lanes % HEAD_DIM < half, -1.0, 1.0)[None, :]]
    reshape x1 -> x0, local copies, waits for them, and re-layouts: 1.29 us -> none  [on_device(): norm_gain.reshape(1, -1)]
where the time goes in v1:
time: 68 us; the launch traced here: 67.9 us
  Pallas kernels  65.3 us (96%)
  local copies, waits for them, and re-layouts  1.94 us (3%)
    pallas_call x1, Pallas kernels, on_device(): call(tokens, norm_gain.reshape(-1, 128), conv_value_weight, conv_gate_wei...  65.3 us
    unnamed x2, local copies, waits for them, and re-layouts  1.94 us

profile of v1, /device:TPU:1, one launch (start us, length us, event | category | flops | bytes accessed | tf_op | source)
XLA Modules:
  0.0 67.9 jit_solution(9337246575391488396)
XLA Ops:
  0.6 65.3 %layer.1 = (bf16[4,128,2048]{2,1,0:T(8,128)(2,1)S(1)}, f32[4,2,1024]{2,1,0:T(2,128)S(1)}) custom-call(bf16[4,1024,2048]{2,1,0:T(8,128)(2,1)} %tokens.1, bf16[16,128]{1,0:T(8,128)(2,1)} %bitcast.6, bf16[128,128]{1,0:T(8,128)(2,1)} %w_value.1, bf16[128,128]{1,0:T(8,128)(2,1)} %w_gate.1, bf16[128,128]{1,0:T(8,128)(2,1)} %w_query.1, bf16[64,128]{1,0:T(8,128)(2,1)} %bitcast.4, ...), custom_call_target="tpu_custom_call" | custom-call | tf_op jit(solution)/shard_map/layer/pallas_call | solution.py:677
  65.9 1.3 %copy.17 = bf16[4,128,2048]{2,1,0:T(8,128)(2,1)} copy(bf16[4,128,2048]{2,1,0:T(8,128)(2,1)S(1)} %get-tuple-element.2) | data formatting | bytes 4194304
  67.3 0.6 copy.18

commit v2 on v1

--- a/solution.py
+++ b/solution.py
@@ -65,6 +65,9 @@
     val_t,
     edges,
     bias,
+    score_buf,
+    weight_buf,
+    partial_out,
     fsend,
     asend,
     cbm,
@@ -81,9 +84,8 @@
     sp, tp = lax.axis_index("sp"), lax.axis_index("tp")
     z, x = sp // X, sp % X
     y, c = tp // CORES, tp % CORES
-    half_y = Y // 2
-    yh, yl = y // half_y, y % half_y
     slot = c * Y + y
+    own_rows = pl.ds(pl.multiple_of(y * 128, 128), 128)
 
     def at_x(d):
         return (z * X + (x + d) % X, tp)
@@ -133,37 +135,45 @@
         group[1].wait_send()
 
     class Ring:
-        def __init__(self, part, me, size, at):
+        def __init__(self, part, whole, me, size, at):
             i = ids(6)
-            ahead, behind = at(1), at(size - 1)
-            lo, hi = part(me, 0), part(me, 1)
-            self.direct = [remote(lo, lo, i, ahead)]
-            self.relayed, self.late = [], [remote(hi, hi, i + 1, ahead)]
+            before, after = (me + size - 1) % size, (me + 1) % size
+
+            def half(n, k, h, d):
+                return group_of(i + n, [(ref, ref, at(d)) for ref in part(k, h)], whole)
+
+            self.direct = [half(0, me, 0, 1)]
+            self.relayed, self.late = [], [half(1, me, 1, 1)]
+            self.passed, self.rest = [], []
             if size == 2:
                 return
-            self.direct.append(remote(hi, hi, i + 2, behind))
-            self.late.append(remote(lo, lo, i + 3, behind))
-            near, far = part((me + size - 1) % size, 0), part((me + 1) % size, 1)
-            self.passed = [near, far]
-            self.rest = [part((me + size - 1) % size, 1), part((me + 1) % size, 0)]
-            self.relayed = [remote(near, near, i + 4, ahead), remote(far, far, i + 5, behind)]
+            self.direct.append(half(2, me, 1, size - 1))
+            self.late.append(half(3, me, 0, size - 1))
+            self.relayed = [half(4, before, 0, 1), half(5, after, 1, size - 1)]
+            self.passed = part(before, 0) + part(after, 1)
+            self.rest = part(before, 1) + part(after, 0)
 
         def begin(self):
-            start(self.direct)
-            start(self.late)
+            for group in self.direct + self.late:
+                start(group[0])
 
         def relay(self):
-            for cp in self.direct:
-                cp.wait_recv()
-            start(self.relayed)
+            for group in self.direct:
+                arrived(group)
+            for group in self.relayed:
+                start(group[0])
+
+        def near(self):
+            for group in self.late:
+                arrived(group)
 
         def finish(self):
-            for cp in self.late + self.relayed:
-                cp.wait_recv()
+            for group in self.relayed:
+                arrived(group)
 
         def drain(self):
-            for cp in self.direct + self.late + self.relayed:
-                cp.wait_send()
+            for group in self.direct + self.late + self.relayed:
+                left_here(group)
 
     def tok_copy(i):
         seq, r = i // per_seq, (i % per_seq) * LN_ROWS
@@ -183,13 +193,12 @@
     for device in greeted:
         pl.semaphore_signal(barrier, inc=1, device_id=device, device_id_type=MESH)
 
-    tile_at = pl.multiple_of(yl * 256, 256)
     wanted = [
         (w_value, w_a.at[z, x, :, pl.ds(0, 128)]),
         (w_gate, w_a.at[z, x, :, pl.ds(128, 128)]),
         (w_query, w_b.at[z, x, :, pl.ds(0, 128)]),
-        (w_oc, o_w.at[c, yh, z, x, pl.ds(tile_at, 128)]),
-        (w_oa, o_w.at[c, yh, z, x, pl.ds(tile_at + 128, 128)]),
+        (w_oc, o_w.at[c, 0, z, x, own_rows]),
+        (w_oa, o_w.at[c, 1, z, x, own_rows]),
         (w_key, key_buf.at[pl.ds(0, 64)]),
         (w_val, key_buf.at[pl.ds(64, 64)]),
         (conv_taps, taps_rows),
@@ -242,29 +251,41 @@
         group_of(ids(1), [(w_a.at[z, x], w_a.at[z, x], at_x(d)) for d in range(1, X)], w_a.at[0, pl.ds(0, X - 1)]),
         group_of(ids(1), [(w_b.at[z, x], w_b.at[z, x], at_z(d)) for d in range(1, Z)], w_b.at[pl.ds(0, Z - 1), 0]),
     ]
+    rows_half = 128 // 2
+
+    def others(block, me, size, h):
+        if size == 2:
+            return [block(1 - me).at[pl.ds(h * rows_half, rows_half)]]
+        opposite = block((me + 2) % size).at[pl.ds(h * rows_half, rows_half)]
+        return [block((me + 1 + 2 * h) % size), opposite]
+
+    half_rows = w_a.at[0, 0, pl.ds(0, rows_half)]
+    most_rows = w_a.at[0, pl.ds(0, X - 1), pl.ds(0, rows_half)]
+    in_own = [
+        Ring(lambda k, h: [w_a.at[k, x, pl.ds(h * rows_half, rows_half)]], half_rows, z, Z, at_z),
+        Ring(lambda k, h: [w_b.at[z, k, pl.ds(h * rows_half, rows_half)]], half_rows, x, X, at_x),
+    ]
     in_2 = [
-        Ring(lambda k, h: w_a.at[k, pl.ds(h * half_x, half_x)], z, Z, at_z),
-        Ring(lambda k, h: w_b.at[pl.ds(h * half_z, half_z), k], x, X, at_x),
+        Ring(lambda k, h: others(lambda n: w_a.at[k, n], x, X, h), most_rows, z, Z, at_z),
+        Ring(lambda k, h: others(lambda n: w_b.at[n, k], z, Z, h), most_rows, x, X, at_x),
     ]
-    tile = o_w.at[c, yh, z, x, pl.ds(tile_at, 256)]
-    out_0 = group_of(ids(1), [(tile, tile, at_y(d)) for d in range(1, Y)], fsend.at[0, pl.ds(0, (Y - 1) * 256)])
     own_gain = gain_all.at[slot]
     gains = group_of(ids(1), [(own_gain, own_gain, at_tp(d)) for d in range(1, TP)], gain_all.at[pl.ds(0, TP - 1)])
+    tile_0, tile_1 = o_w.at[c, 0, z, x, own_rows], o_w.at[c, 1, z, x, own_rows]
+    out_0 = [
+        group_of(ids(1), [(tile_0, tile_0, at_x(d)) for d in range(1, X)], fsend.at[0, pl.ds(0, (X - 1) * 128)]),
+        group_of(ids(1), [(tile_1, tile_1, at_z(d)) for d in range(1, Z)], fsend.at[0, pl.ds(0, (Z - 1) * 128)]),
+    ]
+    row_0, column_1 = o_w.at[c, 0, z, :, own_rows], o_w.at[c, 1, :, x, own_rows]
     out_1 = [
+        group_of(ids(1), [(row_0, row_0, at_y(d)) for d in range(1, Y)], o_w.at[0, 0, 0, :, pl.ds(0, (Y - 1) * 128)]),
         group_of(
-            ids(1),
-            [(o_w.at[c, 0, z, x], o_w.at[c, 0, z, x], at_x(d)) for d in range(1, X)],
-            o_w.at[0, 0, 0, pl.ds(0, X - 1)],
-        ),
-        group_of(
-            ids(1),
-            [(o_w.at[c, 1, z, x], o_w.at[c, 1, z, x], at_z(d)) for d in range(1, Z)],
-            o_w.at[0, 0, pl.ds(0, Z - 1), 0],
+            ids(1), [(column_1, column_1, at_y(d)) for d in range(1, Y)], o_w.at[0, 0, :, 0, pl.ds(0, (Y - 1) * 128)]
         ),
     ]
     out_2 = [
-        Ring(lambda k, h: o_w.at[c, 0, k, pl.ds(h * half_x, half_x)], z, Z, at_z),
-        Ring(lambda k, h: o_w.at[c, 1, pl.ds(h * half_z, half_z), k], x, X, at_x),
+        Ring(lambda k, h: [o_w.at[c, 0, k, pl.ds(h * half_x, half_x)]], o_w.at[0, 0, 0, pl.ds(0, half_x)], z, Z, at_z),
+        Ring(lambda k, h: [o_w.at[c, 1, pl.ds(h * half_z, half_z), k]], o_w.at[0, 0, 0, pl.ds(0, half_x)], x, X, at_x),
     ]
 
     def to_partner(d):
@@ -272,17 +293,17 @@
         return [(row, row, partner), (column, column, partner)]
 
     pair_1 = group_of(ids(1), to_partner(0), o_w.at[0, 0, pl.ds(0, 2)])
+    pairs = [pair_1]
     if X == 2:
-        early, late = [], to_partner(1)
-        late_whole = o_w.at[0, 0, pl.ds(0, 2)]
+        pair_4 = group_of(ids(1), to_partner(1), o_w.at[0, 0, pl.ds(0, 2)])
+        pairs += [pair_4]
     else:
-        passed = [ref for ring in out_2 for ref in ring.passed]
-        early = [(ref, ref, partner) for ref in passed]
-        rest = [ref for ring in out_2 for ref in ring.rest]
-        late = [(ref, ref, partner) for ref in rest] + to_partner(2)
-        late_whole = o_w.at[0, 0]
-    pair_2 = group_of(ids(1), early, o_w.at[0, 0, pl.ds(0, 2)])
-    pair_3 = group_of(ids(1), late, late_whole)
+        passed = [(ref, ref, partner) for ring in out_2 for ref in ring.passed]
+        rest = [(ref, ref, partner) for ring in out_2 for ref in ring.rest]
+        pair_2 = group_of(ids(1), passed, o_w.at[0, 0, pl.ds(0, 2)])
+        pair_3 = group_of(ids(1), rest, o_w.at[0, 0, pl.ds(0, 2)])
+        pair_4 = group_of(ids(1), to_partner(2), o_w.at[0, 0, pl.ds(0, 2)])
+        pairs += [pair_2, pair_3, pair_4]
 
     rim_i, keys_i = ids(SEQS), ids(SEQS)
 
@@ -310,7 +331,7 @@
         return pl.ds(pl.multiple_of(device_tp * 128, 128), 128)
 
     conv_lanes = pl.ds(pl.multiple_of(slot * 128, 128), 128)
-    attn_lanes = pl.ds(pl.multiple_of(slot * 256 + 128, 128), 128)
+    attn_lanes = pl.ds(pl.multiple_of(c * (Y * 256) + (Y + y) * 128, 128), 128)
 
     def conv_out_copies(s):
         return group_of(
@@ -338,8 +359,8 @@
         pl.semaphore_wait(barrier, len(greeted))
     for group in in_1:
         start(group[0])
-    start(out_0[0])
-    start(gains[0])
+    for ring in in_own:
+        ring.begin()
 
     def ln_block(i, carry):
         tok_copy(i).wait()
@@ -360,27 +381,37 @@
 
         return lax.fori_loop(0, LN_ROWS // 16, group, carry, unroll=16)
 
-    cuts = (0, n_blocks * 3 // 8, n_blocks * 7 // 8, n_blocks)
-    with jax.named_scope("norm_a"):
-        lax.fori_loop(cuts[0], cuts[1], ln_block, 0)
+    def norm_blocks(first, last):
+        with jax.named_scope("norm"):
+            lax.fori_loop(n_blocks * first // 16, n_blocks * last // 16, ln_block, 0)
+
+    norm_blocks(0, 2)
+    for group in out_0:
+        start(group[0])
+    start(gains[0])
+    norm_blocks(2, 6)
     with jax.named_scope("wait_in_1"):
         for group in in_1:
             arrived(group)
     for ring in in_2:
         ring.begin()
-    with jax.named_scope("norm_b"):
-        lax.fori_loop(cuts[1], cuts[2], ln_block, 0)
+    with jax.named_scope("wait_own"):
+        for ring in in_own:
+            ring.relay()
+    norm_blocks(6, 9)
+    with jax.named_scope("wait_out_0"):
+        for group in out_0:
+            arrived(group)
+    for group in out_1:
+        start(group[0])
+    norm_blocks(9, 13)
     with jax.named_scope("wait_relay"):
         for ring in in_2:
             ring.relay()
-    with jax.named_scope("wait_out_0"):
-        arrived(out_0)
-    for group in out_1:
-        start(group[0])
-    with jax.named_scope("norm_c"):
-        lax.fori_loop(cuts[2], cuts[3], ln_block, 0)
+    norm_blocks(13, 16)
     with jax.named_scope("wait_in_2"):
-        for ring in in_2:
+        for ring in in_own + in_2:
+            ring.near()
             ring.finish()
 
     lane = lax.broadcasted_iota(jnp.int32, (1, 128), 1)
@@ -444,46 +475,33 @@
         start(conv_out_copies(s)[0])
         cbm[s, :, conv_lanes] = fsend[s, rows_of(tp), :]
 
-    def project_edges(s, carry):
-        project(s, (0, T - 128))
+    def project_edges(k, carry):
+        for s in (2 * k, 2 * k + 1):
+            project(s, (0, T - 128))
+        for s in (2 * k, 2 * k + 1):
+            start(rims(s)[0])
+        for s in (2 * k, 2 * k + 1):
+            start(edge_keys(s)[0])
         return carry
 
-    def send_edges(s, carry):
-        start(edge_keys(s)[0])
-        start(rims(s)[0])
-        return carry
-
-    def project_inner(k, carry):
-        inner = T // 256 - 1
-        project(k // inner, (128 + (k % inner) * 256,))
-        return carry
-
-    n_inner = SEQS * (T // 256 - 1)
-    inner_cut = n_inner // 2
+    inner = T // 256 - 1
+
     with jax.named_scope("project_edges"):
-        lax.fori_loop(0, SEQS, project_edges, 0, unroll=2)
-    lax.fori_loop(0, SEQS, send_edges, 0)
-    with jax.named_scope("project_a"):
-        lax.fori_loop(0, inner_cut, project_inner, 0, unroll=3)
+        lax.fori_loop(0, SEQS // 2, project_edges, 0)
     with jax.named_scope("wait_out_1"):
         for group in out_1:
             arrived(group)
-    with jax.named_scope("wait_rims"):
-        for ring in out_2:
-            ring.begin()
+    for ring in out_2:
+        ring.begin()
     start(pair_1[0])
-    with jax.named_scope("project_b"):
-        lax.fori_loop(inner_cut, n_inner, project_inner, 0, unroll=3)
-
-    def each_convolve(s, carry):
-        convolve(s)
-        return carry
-
-    lax.fori_loop(0, SEQS, each_convolve, 0)
-    with jax.named_scope("wait_out_relay"):
-        for ring in out_2:
-            ring.relay()
-    start(pair_2[0])
+
+    def project_inner(s):
+        def step(k, carry):
+            project(s, (128 + k * 256,))
+            return carry
+
+        with jax.named_scope("project"):
+            lax.fori_loop(0, inner, step, 0, unroll=inner)
 
     head_lane = lax.broadcasted_iota(jnp.int32, (1, 256), 1)
     sink_row = jnp.where(head_lane < 128, sink[0], sink[1])
@@ -493,48 +511,89 @@
         kpad[s, pl.ds(first, WINDOW), :] = jnp.where(low_head, kv, pltpu.roll(kv, 64, 1)).astype(BF16)
         val_t[s, :, pl.ds(first, WINDOW)] = edges[s, e].T[64:]
 
-    def attend(s, carry):
+    blocks = T // 128
+
+    def attend(s):
+        with jax.named_scope("wait_keys"):
+            arrived(edge_keys(s))
+        widen(s, 0, 0)
+        widen(s, 3, WINDOW + T)
+
+        tops, totals = {}, {}
+
+        def score(b):
+            keys = kpad[s, pl.ds(b * 128, 384), :]
+            scores = dot(keys, qz[s, b].reshape(256, 128), ((1,), (1,)))
+            low, high = bias[0], bias[1]
+            if b == 0:
+                low = low + jnp.where(sp == 0, MASK_VALUE, 0.0)
+            if b == blocks - 1:
+                high = high + jnp.where(sp == NSP - 1, MASK_VALUE, 0.0)
+            s_0, s_1, s_2 = scores[:128] + low, scores[128:256], scores[256:] + high
+            top = jnp.max(jnp.maximum(jnp.maximum(s_0, s_1), s_2), axis=0, keepdims=True)
+            tops[b] = jnp.maximum(top, sink_row)
+            for n, part in enumerate((s_0, s_1, s_2)):
+                score_buf[b % 2, n] = part
+
+        def weigh(b):
+            top = tops[b]
+            e_0, e_1, e_2 = (jnp.exp(score_buf[b % 2, n] - top) for n in range(3))
+            total = jnp.sum(e_0 + e_1 + e_2, axis=0, keepdims=True) + jnp.exp(sink_row - top)
+            totals[b] = total
+            logs = top + jnp.log(total)
+            log_total[s, :, pl.ds(b * 128, 128)] = jnp.concatenate([logs[:, :128], logs[:, 128:]], axis=0)
+            for n, part in enumerate((e_0, e_1, e_2)):
+                weight_buf[b % 2, n] = part.astype(BF16)
+
+        def collect(b):
+            weights = weight_buf[b % 2].reshape(384, 256)
+            out = dot(val_t[s, :, pl.ds(b * 128, 384)], weights) * (1.0 / totals[b])
+            both = jnp.concatenate([out[:, :128], out[:, 128:]], axis=0)
+            asend[s, pl.ds(b * 128, 128), :] = both.astype(BF16).T
+
+        with jax.named_scope("attend"):
+            for b in range(blocks + 2):
+                if b < blocks:
+                    score(b)
+                if 0 <= b - 1 < blocks:
+                    weigh(b - 1)
+                if b >= 2:
+                    collect(b - 2)
+        start(attn_out_copies(s)[0])
+        bm[s, :, attn_lanes] = asend[s, rows_of(tp), :]
+
+    def sequence(s, carry):
+        project_inner(s)
+
         @pl.when(s == SEQS - 1)
         def _():
             with jax.named_scope("wait_out_2"):
                 for ring in out_2:
                     ring.finish()
-            start(pair_3[0])
-
-        with jax.named_scope("wait_keys"):
-            arrived(edge_keys(s))
-        widen(s, 0, 0)
-        widen(s, 3, WINDOW + T)
-
-        def block(b, carry):
-            r = pl.multiple_of(b * 128, 128)
-            keys = kpad[s, pl.ds(r, 384), :]
-            scores = dot(keys, qz[s, b].reshape(256, 128), ((1,), (1,)))
-            off_left = jnp.where((sp == 0) & (b == 0), MASK_VALUE, 0.0)
-            off_right = jnp.where((sp == NSP - 1) & (b == T // 128 - 1), MASK_VALUE, 0.0)
-            s_0 = scores[:128] + (bias[0] + off_left)
-            s_1 = scores[128:256]
-            s_2 = scores[256:] + (bias[1] + off_right)
-            top = jnp.max(jnp.maximum(jnp.maximum(s_0, s_1), s_2), axis=0, keepdims=True)
-            top = jnp.maximum(top, sink_row)
-            e_0, e_1, e_2 = jnp.exp(s_0 - top), jnp.exp(s_1 - top), jnp.exp(s_2 - top)
-            total = jnp.sum(e_0 + e_1 + e_2, axis=0, keepdims=True) + jnp.exp(sink_row - top)
-            logs = top + jnp.log(total)
-            log_total[s, :, pl.ds(r, 128)] = jnp.concatenate([logs[:, :128], logs[:, 128:]], axis=0)
-            weights = jnp.concatenate([e_0.astype(BF16), e_1.astype(BF16), e_2.astype(BF16)], axis=0)
-            out = dot(val_t[s, :, pl.ds(r, 384)], weights) * (1.0 / total)
-            both = jnp.concatenate([out[:, :128], out[:, 128:]], axis=0)
-            asend[s, pl.ds(r, 128), :] = both.astype(BF16).T
-            return carry
-
-        with jax.named_scope("attend"):
-            lax.fori_loop(0, T // 128, block, 0, unroll=min(8, T // 128))
-        start(attn_out_copies(s)[0])
-        bm[s, :, attn_lanes] = asend[s, rows_of(tp), :]
+            start(pair_4[0])
+
+        convolve(s)
+
+        @pl.when(s == min(1, SEQS - 1))
+        def _():
+            with jax.named_scope("wait_out_relay"):
+                for ring in out_2:
+                    ring.relay()
+            if X > 2:
+                start(pair_2[0])
+
+        @pl.when(s == min(2, SEQS - 1))
+        def _():
+            with jax.named_scope("wait_out_near"):
+                for ring in out_2:
+                    ring.near()
+            if X > 2:
+                start(pair_3[0])
+
+        attend(s)
         return carry
 
-    lax.fori_loop(0, SEQS, attend, 0)
-
+    lax.fori_loop(0, SEQS, sequence, 0)
     arrived(gains)
 
     def finish(s):
@@ -550,49 +609,73 @@
             scale = lax.rsqrt(var + EPSILON)
             for n in range(TP):
                 u = centred[:, n * 128 : (n + 1) * 128] * scale * gain_all[n, 0:1, :]
-                bm[s, at, n * 256 : n * 256 + 128] = jax.nn.silu(u).astype(BF16)
+                first = n // Y * (Y * 256) + n % Y * 128
+                bm[s, at, first : first + 128] = jax.nn.silu(u).astype(BF16)
             return carry
 
         with jax.named_scope("channel_norm"):
             lax.fori_loop(0, 128 // 16, group, 0, unroll=8)
 
-    def out_rows(s, carry):
-        finish(2 * s)
-        finish(2 * s + 1)
-        with jax.named_scope("wait_attn"):
-            arrived(attn_out_copies(2 * s))
-            arrived(attn_out_copies(2 * s + 1))
-
-        @pl.when(s == 0)
-        def _():
+    def out_columns(p, h):
+        zz, xx = p // (X // 2), (p % (X // 2)) * 2
+        pieces = [
+            jnp.concatenate([o_w[cc, hh, zz, xx], o_w[cc, hh, zz, xx + 1]], axis=1)
+            for cc in range(CORES)
+            for hh in h
+        ]
+        return jnp.concatenate(pieces, axis=0)
+
+    columns_of = lambda p: pl.ds(pl.multiple_of(p * 256, 256), 256)
+    first_rows = SEQS // 2
+
+    for s in range(SEQS):
+        finish(s)
+        if s == first_rows - 1:
             with jax.named_scope("wait_pair"):
-                arrived(pair_1)
-                if X > 2:
-                    arrived(pair_2)
-                arrived(pair_3)
-
-        def out_project(p, carry):
-            zz, xx = p // (X // 2), (p % (X // 2)) * 2
-            pieces = [
-                jnp.concatenate([o_w[cc, hh, zz, xx], o_w[cc, hh, zz, xx + 1]], axis=1)
-                for cc in range(CORES)
-                for hh in range(2)
-            ]
-            rows = bm[pl.ds(2 * s, 2)].reshape(256, TP * 256)
-            acc = dot(rows, jnp.concatenate(pieces, axis=0))
-            columns = pl.ds(pl.multiple_of(p * 256, 256), 256)
-            mixed[pl.ds(2 * s, 2), :, columns] = acc.astype(BF16).reshape(2, 128, 256)
-            return carry
-
-        with jax.named_scope("out_project"):
-            lax.fori_loop(0, NSP // 2, out_project, 0, unroll=2)
+                for group in pairs:
+                    arrived(group)
+            with jax.named_scope("wait_attn"):
+                for n in range(first_rows):
+                    arrived(attn_out_copies(n))
+
+            def out_whole(p, carry):
+                rows = bm[:first_rows].reshape(first_rows * 128, TP * 256)
+                acc = dot(rows, out_columns(p, (0, 1)))
+                mixed[:first_rows, :, columns_of(p)] = acc.astype(BF16).reshape(first_rows, 128, 256)
+                return carry
+
+            with jax.named_scope("out_whole"):
+                lax.fori_loop(0, NSP // 2, out_whole, 0, unroll=2)
+
+    n_late = SEQS - first_rows
+    branch = Y * 128
+
+    def late_rows(h):
+        first = [(2 * cc + h) * branch for cc in range(CORES)]
+        lanes = [bm[first_rows:, :, k : k + branch].reshape(n_late * 128, branch) for k in first]
+        return jnp.concatenate(lanes, axis=1)
+
+    def out_conv(p, carry):
+        partial_out[p] = dot(late_rows(0), out_columns(p, (0,)))
         return carry
 
-    lax.fori_loop(0, SEQS // 2, out_rows, 0)
-
-    for group in in_1 + [out_0, gains] + out_1 + [pair_1, pair_3] + ([pair_2] if X > 2 else []):
+    with jax.named_scope("out_conv"):
+        lax.fori_loop(0, NSP // 2, out_conv, 0, unroll=2)
+    with jax.named_scope("wait_attn"):
+        for n in range(first_rows, SEQS):
+            arrived(attn_out_copies(n))
+
+    def out_attn(p, carry):
+        acc = partial_out[p] + dot(late_rows(1), out_columns(p, (1,)))
+        mixed[first_rows:, :, columns_of(p)] = acc.astype(BF16).reshape(n_late, 128, 256)
+        return carry
+
+    with jax.named_scope("out_attn"):
+        lax.fori_loop(0, NSP // 2, out_attn, 0, unroll=2)
+
+    for group in in_1 + [gains] + out_0 + out_1 + pairs:
         left_here(group)
-    for ring in in_2 + out_2:
+    for ring in in_own + in_2 + out_2:
         ring.drain()
 
     def drain(s, carry):
@@ -627,7 +710,7 @@
     angles = np.concatenate(parts)[:, None] * np.tile(inverse.astype(np.float64), 4)[None, :]
     turns = np.stack([np.cos(angles), np.sin(angles)]).astype(np.float32)
 
-    n_copies = 2 + 12 + 2 + 2 + 12 + 3 + 4 * seqs
+    n_copies = 2 + 24 + 2 + 2 + 1 + 12 + 4 + 4 * seqs
     vmem = pl.BlockSpec(memory_space=pltpu.VMEM)
     far = pl.BlockSpec(memory_space=pl.ANY)
     call = pl.pallas_call(
@@ -644,7 +727,7 @@
             pltpu.VMEM((seqs * toks, width), BF16),
             pltpu.VMEM((zs, xs, 128, 256), BF16),
             pltpu.VMEM((zs, xs, 128, 256), BF16),
-            pltpu.VMEM((CORES, 2, zs, xs, ys // 2 * 256, 128), BF16),
+            pltpu.VMEM((CORES, 2, zs, xs, ys * 128, 128), BF16),
             pltpu.VMEM((tps, 8, 128), F32),
             pltpu.VMEM((31, 128), F32),
             pltpu.VMEM((128, 128), BF16),
@@ -660,6 +743,9 @@
             pltpu.VMEM((seqs, HEAD_DIM, toks + 2 * WINDOW), BF16),
             pltpu.VMEM((seqs, 4, WINDOW, 128), BF16),
             pltpu.VMEM((2, WINDOW, 256), F32),
+            pltpu.VMEM((2, 3, WINDOW, 256), F32),
+            pltpu.VMEM((2, 3, WINDOW, 256), BF16),
+            pltpu.VMEM((xs * zs // 2, seqs // 2 * 128, 256), F32),
             pltpu.VMEM((seqs, toks, 128), BF16),
             pltpu.VMEM((seqs, toks, 128), BF16),
             pltpu.VMEM((seqs, toks // tps, tps * 128), BF16),

time: 68 us -> 65.3 us (0.960)
  Pallas kernels: 65.3 us -> 62.6 us
    pallas_call x1, Pallas kernels: 65.3 us -> 62.6 us  [on_device(): call(tokens, norm_gain.reshape(-1, 128), conv_value_weight, conv_gate_wei...]
where the time goes in v2:
time: 65.3 us; the launch traced here: 65.1 us
  Pallas kernels  62.6 us (96%)
  local copies, waits for them, and re-layouts  1.94 us (3%)
    pallas_call x1, Pallas kernels, on_device(): call(tokens, norm_gain.reshape(-1, 128), conv_value_weight, conv_gate_wei...  62.6 us
    unnamed x2, local copies, waits for them, and re-layouts  1.94 us

profile of v2, /device:TPU:1, one launch (start us, length us, event | category | flops | bytes accessed | tf_op | source)
XLA Modules:
  0.0 65.1 jit_solution(15717813901795246482)
XLA Ops:
  0.6 62.6 %layer.1 = (bf16[4,128,2048]{2,1,0:T(8,128)(2,1)S(1)}, f32[4,2,1024]{2,1,0:T(2,128)S(1)}) custom-call(bf16[4,1024,2048]{2,1,0:T(8,128)(2,1)} %tokens.1, bf16[16,128]{1,0:T(8,128)(2,1)} %bitcast.6, bf16[128,128]{1,0:T(8,128)(2,1)} %w_value.1, bf16[128,128]{1,0:T(8,128)(2,1)} %w_gate.1, bf16[128,128]{1,0:T(8,128)(2,1)} %w_query.1, bf16[64,128]{1,0:T(8,128)(2,1)} %bitcast.4, ...), custom_call_target="tpu_custom_call" | custom-call | tf_op jit(solution)/shard_map/layer/pallas_call | solution.py:763
  63.2 1.3 %copy.17 = bf16[4,128,2048]{2,1,0:T(8,128)(2,1)} copy(bf16[4,128,2048]{2,1,0:T(8,128)(2,1)S(1)} %get-tuple-element.2) | data formatting | bytes 4194304
  64.5 0.6 copy.18

commit v3 on v2

--- a/solution.py
+++ b/solution.py
@@ -1,4 +1,5 @@
 import functools
+import math
 
 import jax
 import jax.numpy as jnp
@@ -110,11 +111,11 @@
         counter[0] += n
         return first
 
-    def remote(src, dst, i, device):
+    def remote(src, dst, i, device, sent=0):
         return pltpu.make_async_remote_copy(
             src_ref=src,
             dst_ref=dst,
-            send_sem=send_sem.at[i],
+            send_sem=send_sem.at[sent],
             recv_sem=recv_sem.at[i],
             device_id=device,
             device_id_type=MESH,
@@ -124,15 +125,12 @@
         for cp in copies:
             cp.start()
 
-    def group_of(i, pairs, whole):
-        copies = [remote(src, dst, i, device) for src, dst, device in pairs]
-        return copies, remote(whole, whole, i, right)
+    def group_of(i, pairs, whole, sent=0):
+        copies = [remote(src, dst, i, device, sent) for src, dst, device in pairs]
+        return copies, remote(whole, whole, i, right, sent), math.prod(whole.shape) * whole.dtype.itemsize
 
     def arrived(group):
         group[1].wait_recv()
-
-    def left_here(group):
-        group[1].wait_send()
 
     class Ring:
         def __init__(self, part, whole, me, size, at):
@@ -154,7 +152,15 @@
             self.rest = part(before, 1) + part(after, 0)
 
         def begin(self):
-            for group in self.direct + self.late:
+            self.begin_direct()
+            self.begin_late()
+
+        def begin_direct(self):
+            for group in self.direct:
+                start(group[0])
+
+        def begin_late(self):
+            for group in self.late:
                 start(group[0])
 
         def relay(self):
@@ -171,9 +177,8 @@
             for group in self.relayed:
                 arrived(group)
 
-        def drain(self):
-            for group in self.direct + self.late + self.relayed:
-                left_here(group)
+        def groups(self):
+            return self.direct + self.late + self.relayed
 
     def tok_copy(i):
         seq, r = i // per_seq, (i % per_seq) * LN_ROWS
@@ -213,6 +218,128 @@
 
     for n in range(SLOTS - 1):
         tok_copy(n).start()
+
+    half_x, half_z = X // 2, Z // 2
+
+    def others(block, me, size, h):
+        if size == 2:
+            return [block(1 - me).at[pl.ds(h * 32, 32)]]
+        opposite = block((me + 2) % size).at[pl.ds(h * 32, 32)]
+        return [block((me + 1 + 2 * h) % size), opposite]
+
+    def gather_of(w):
+        mine = [w.at[z, x, pl.ds(64 * f, 64)] for f in range(2)]
+        first = [
+            group_of(ids(1), [(mine[0], mine[0], at_x(d)) for d in range(1, X)], w.at[0, pl.ds(0, X - 1), pl.ds(0, 64)]),
+            group_of(ids(1), [(mine[1], mine[1], at_z(d)) for d in range(1, Z)], w.at[pl.ds(0, Z - 1), 0, pl.ds(0, 64)]),
+        ]
+        own = [
+            Ring(lambda k, h: [w.at[k, x, pl.ds(h * 32, 32)]], w.at[0, 0, pl.ds(0, 32)], z, Z, at_z),
+            Ring(lambda k, h: [w.at[z, k, pl.ds(64 + h * 32, 32)]], w.at[0, 0, pl.ds(0, 32)], x, X, at_x),
+        ]
+        most = w.at[0, pl.ds(0, X - 1), pl.ds(0, 32)]
+        rest = [
+            Ring(lambda k, h: others(lambda n: w.at[k, n, pl.ds(0, 64)], x, X, h), most, z, Z, at_z),
+            Ring(lambda k, h: others(lambda n: w.at[n, k, pl.ds(64, 64)], z, Z, h), most, x, X, at_x),
+        ]
+        return first, own, rest
+
+    first_a, own_a, rest_a = gather_of(w_a)
+    first_b, own_b, rest_b = gather_of(w_b)
+    own_gain = gain_all.at[slot]
+    gains = group_of(ids(1), [(own_gain, own_gain, at_tp(d)) for d in range(1, TP)], gain_all.at[pl.ds(0, TP - 1)], 1)
+    tile_0, tile_1 = o_w.at[c, 0, z, x, own_rows], o_w.at[c, 1, z, x, own_rows]
+    out_0 = [
+        group_of(ids(1), [(tile_0, tile_0, at_x(d)) for d in range(1, X)], fsend.at[0, pl.ds(0, (X - 1) * 128)]),
+        group_of(ids(1), [(tile_1, tile_1, at_z(d)) for d in range(1, Z)], fsend.at[0, pl.ds(0, (Z - 1) * 128)]),
+    ]
+    def rows_from(k):
+        return pl.ds(pl.multiple_of(k * 128, 128), 128)
+
+    quarter = o_w.at[0, 0, 0, pl.ds(0, half_x), pl.ds(0, 128)]
+    out_1 = [
+        Ring(lambda k, h: [o_w.at[c, 0, z, pl.ds(h * half_x, half_x), rows_from(k)]], quarter, y, Y, at_y),
+        Ring(lambda k, h: [o_w.at[c, 1, pl.ds(h * half_z, half_z), x, rows_from(k)]], quarter, y, Y, at_y),
+    ]
+    out_2 = [
+        Ring(lambda k, h: [o_w.at[c, 0, k, pl.ds(h * half_x, half_x)]], o_w.at[0, 0, 0, pl.ds(0, half_x)], z, Z, at_z),
+        Ring(lambda k, h: [o_w.at[c, 1, pl.ds(h * half_z, half_z), k]], o_w.at[0, 0, 0, pl.ds(0, half_x)], x, X, at_x),
+    ]
+
+    def to_partner(d):
+        row, column = o_w.at[c, 0, (z + d) % Z], o_w.at[c, 1, :, (x + d) % X]
+        return [(row, row, partner), (column, column, partner)]
+
+    pair_1 = group_of(ids(1), to_partner(0), o_w.at[0, 0, pl.ds(0, 2)])
+    pairs = [pair_1]
+    if X == 2:
+        pair_4 = group_of(ids(1), to_partner(1), o_w.at[0, 0, pl.ds(0, 2)])
+        pairs += [pair_4]
+    else:
+        passed = [(ref, ref, partner) for ring in out_2 for ref in ring.passed]
+        rest = [(ref, ref, partner) for ring in out_2 for ref in ring.rest]
+        pair_2 = group_of(ids(1), passed, o_w.at[0, 0, pl.ds(0, 2)])
+        pair_3 = group_of(ids(1), rest, o_w.at[0, 0, pl.ds(0, 2)])
+        pair_4 = group_of(ids(1), to_partner(2), o_w.at[0, 0, pl.ds(0, 2)])
+        pairs += [pair_2, pair_3, pair_4]
+
+    rim_i, keys_i = ids(SEQS), ids(SEQS)
+
+    def rims(s):
+        return group_of(
+            rim_i + s,
+            [
+                (gpad.at[s, pl.ds(RIM, RIM)], gpad.at[s, pl.ds(RIM + T, RIM)], left),
+                (gpad.at[s, pl.ds(T, RIM)], gpad.at[s, pl.ds(0, RIM)], right),
+            ],
+            gpad.at[0, pl.ds(0, 2 * RIM)],
+        )
+
+    def edge_keys(s):
+        return group_of(
+            keys_i + s,
+            [(edges.at[s, 1], edges.at[s, 3], left), (edges.at[s, 2], edges.at[s, 0], right)],
+            edges.at[0, pl.ds(0, 2)],
+        )
+
+    conv_i, attn_i = ids(SEQS), ids(SEQS)
+    peers_rows = fsend.at[0, pl.ds(0, (TP - 1) * 128)]
+
+    def rows_of(device_tp):
+        return pl.ds(pl.multiple_of(device_tp * 128, 128), 128)
+
+    conv_lanes = pl.ds(pl.multiple_of(slot * 128, 128), 128)
+    attn_lanes = pl.ds(pl.multiple_of(c * (Y * 256) + (Y + y) * 128, 128), 128)
+
+    def conv_out_copies(s):
+        return group_of(
+            conv_i + s,
+            [
+                (fsend.at[s, rows_of((tp + d) % TP)], cbm.at[s, :, conv_lanes], at_tp(d))
+                for d in range(1, TP)
+            ],
+            peers_rows,
+        )
+
+    def attn_out_copies(s):
+        return group_of(
+            attn_i + s,
+            [
+                (asend.at[s, rows_of((tp + d) % TP)], bm.at[s, :, attn_lanes], at_tp(d))
+                for d in range(1, TP)
+            ],
+            peers_rows,
+        )
+
+    for n in range(2):
+        loads[n].wait()
+    with jax.named_scope("greet"):
+        pl.semaphore_wait(barrier, len(greeted))
+    for group in first_a:
+        start(group[0])
+    for ring in own_a:
+        ring.begin()
+
     for n in (8, 9, 10):
         loads[n].wait()
     run = turn_buf.shape[1] - NSP - 32
@@ -245,122 +372,8 @@
     query_i = lax.broadcasted_iota(jnp.int32, (WINDOW, 256), 1) % WINDOW
     bias[0] = jnp.where(key_i >= query_i, 0.0, MASK_VALUE)
     bias[1] = jnp.where(key_i <= query_i, 0.0, MASK_VALUE)
-
-    half_x, half_z = X // 2, Z // 2
-    in_1 = [
-        group_of(ids(1), [(w_a.at[z, x], w_a.at[z, x], at_x(d)) for d in range(1, X)], w_a.at[0, pl.ds(0, X - 1)]),
-        group_of(ids(1), [(w_b.at[z, x], w_b.at[z, x], at_z(d)) for d in range(1, Z)], w_b.at[pl.ds(0, Z - 1), 0]),
-    ]
-    rows_half = 128 // 2
-
-    def others(block, me, size, h):
-        if size == 2:
-            return [block(1 - me).at[pl.ds(h * rows_half, rows_half)]]
-        opposite = block((me + 2) % size).at[pl.ds(h * rows_half, rows_half)]
-        return [block((me + 1 + 2 * h) % size), opposite]
-
-    half_rows = w_a.at[0, 0, pl.ds(0, rows_half)]
-    most_rows = w_a.at[0, pl.ds(0, X - 1), pl.ds(0, rows_half)]
-    in_own = [
-        Ring(lambda k, h: [w_a.at[k, x, pl.ds(h * rows_half, rows_half)]], half_rows, z, Z, at_z),
-        Ring(lambda k, h: [w_b.at[z, k, pl.ds(h * rows_half, rows_half)]], half_rows, x, X, at_x),
-    ]
-    in_2 = [
-        Ring(lambda k, h: others(lambda n: w_a.at[k, n], x, X, h), most_rows, z, Z, at_z),
-        Ring(lambda k, h: others(lambda n: w_b.at[n, k], z, Z, h), most_rows, x, X, at_x),
-    ]
-    own_gain = gain_all.at[slot]
-    gains = group_of(ids(1), [(own_gain, own_gain, at_tp(d)) for d in range(1, TP)], gain_all.at[pl.ds(0, TP - 1)])
-    tile_0, tile_1 = o_w.at[c, 0, z, x, own_rows], o_w.at[c, 1, z, x, own_rows]
-    out_0 = [
-        group_of(ids(1), [(tile_0, tile_0, at_x(d)) for d in range(1, X)], fsend.at[0, pl.ds(0, (X - 1) * 128)]),
-        group_of(ids(1), [(tile_1, tile_1, at_z(d)) for d in range(1, Z)], fsend.at[0, pl.ds(0, (Z - 1) * 128)]),
-    ]
-    row_0, column_1 = o_w.at[c, 0, z, :, own_rows], o_w.at[c, 1, :, x, own_rows]
-    out_1 = [
-        group_of(ids(1), [(row_0, row_0, at_y(d)) for d in range(1, Y)], o_w.at[0, 0, 0, :, pl.ds(0, (Y - 1) * 128)]),
-        group_of(
-            ids(1), [(column_1, column_1, at_y(d)) for d in range(1, Y)], o_w.at[0, 0, :, 0, pl.ds(0, (Y - 1) * 128)]
-        ),
-    ]
-    out_2 = [
-        Ring(lambda k, h: [o_w.at[c, 0, k, pl.ds(h * half_x, half_x)]], o_w.at[0, 0, 0, pl.ds(0, half_x)], z, Z, at_z),
-        Ring(lambda k, h: [o_w.at[c, 1, pl.ds(h * half_z, half_z), k]], o_w.at[0, 0, 0, pl.ds(0, half_x)], x, X, at_x),
-    ]
-
-    def to_partner(d):
-        row, column = o_w.at[c, 0, (z + d) % Z], o_w.at[c, 1, :, (x + d) % X]
-        return [(row, row, partner), (column, column, partner)]
-
-    pair_1 = group_of(ids(1), to_partner(0), o_w.at[0, 0, pl.ds(0, 2)])
-    pairs = [pair_1]
-    if X == 2:
-        pair_4 = group_of(ids(1), to_partner(1), o_w.at[0, 0, pl.ds(0, 2)])
-        pairs += [pair_4]
-    else:
-        passed = [(ref, ref, partner) for ring in out_2 for ref in ring.passed]
-        rest = [(ref, ref, partner) for ring in out_2 for ref in ring.rest]
-        pair_2 = group_of(ids(1), passed, o_w.at[0, 0, pl.ds(0, 2)])
-        pair_3 = group_of(ids(1), rest, o_w.at[0, 0, pl.ds(0, 2)])
-        pair_4 = group_of(ids(1), to_partner(2), o_w.at[0, 0, pl.ds(0, 2)])
-        pairs += [pair_2, pair_3, pair_4]
-
-    rim_i, keys_i = ids(SEQS), ids(SEQS)
-
-    def rims(s):
-        return group_of(
-            rim_i + s,
-            [
-                (gpad.at[s, pl.ds(RIM, RIM)], gpad.at[s, pl.ds(RIM + T, RIM)], left),
-                (gpad.at[s, pl.ds(T, RIM)], gpad.at[s, pl.ds(0, RIM)], right),
-            ],
-            gpad.at[0, pl.ds(0, 2 * RIM)],
-        )
-
-    def edge_keys(s):
-        return group_of(
-            keys_i + s,
-            [(edges.at[s, 1], edges.at[s, 3], left), (edges.at[s, 2], edges.at[s, 0], right)],
-            edges.at[0, pl.ds(0, 2)],
-        )
-
-    conv_i, attn_i = ids(SEQS), ids(SEQS)
-    peers_rows = fsend.at[0, pl.ds(0, (TP - 1) * 128)]
-
-    def rows_of(device_tp):
-        return pl.ds(pl.multiple_of(device_tp * 128, 128), 128)
-
-    conv_lanes = pl.ds(pl.multiple_of(slot * 128, 128), 128)
-    attn_lanes = pl.ds(pl.multiple_of(c * (Y * 256) + (Y + y) * 128, 128), 128)
-
-    def conv_out_copies(s):
-        return group_of(
-            conv_i + s,
-            [
-                (fsend.at[s, rows_of((tp + d) % TP)], cbm.at[s, :, conv_lanes], at_tp(d))
-                for d in range(1, TP)
-            ],
-            peers_rows,
-        )
-
-    def attn_out_copies(s):
-        return group_of(
-            attn_i + s,
-            [
-                (asend.at[s, rows_of((tp + d) % TP)], bm.at[s, :, attn_lanes], at_tp(d))
-                for d in range(1, TP)
-            ],
-            peers_rows,
-        )
-
-    for n in range(5):
+    for n in range(2, 5):
         loads[n].wait()
-    with jax.named_scope("greet"):
-        pl.semaphore_wait(barrier, len(greeted))
-    for group in in_1:
-        start(group[0])
-    for ring in in_own:
-        ring.begin()
 
     def ln_block(i, carry):
         tok_copy(i).wait()
@@ -386,31 +399,43 @@
             lax.fori_loop(n_blocks * first // 16, n_blocks * last // 16, ln_block, 0)
 
     norm_blocks(0, 2)
-    for group in out_0:
+    for group in first_b + out_0 + [gains]:
         start(group[0])
-    start(gains[0])
-    norm_blocks(2, 6)
+    norm_blocks(2, 5)
     with jax.named_scope("wait_in_1"):
-        for group in in_1:
+        for group in first_a:
             arrived(group)
-    for ring in in_2:
+    for ring in rest_a:
         ring.begin()
     with jax.named_scope("wait_own"):
-        for ring in in_own:
+        for ring in own_a:
             ring.relay()
-    norm_blocks(6, 9)
+    for ring in own_b:
+        ring.begin()
+    norm_blocks(5, 7)
+    with jax.named_scope("wait_in_b1"):
+        for group in first_b:
+            arrived(group)
+    for ring in rest_b:
+        ring.begin()
+    norm_blocks(7, 9)
     with jax.named_scope("wait_out_0"):
         for group in out_0:
             arrived(group)
-    for group in out_1:
-        start(group[0])
-    norm_blocks(9, 13)
+    for ring in out_1:
+        ring.begin_direct()
+    for ring in out_1:
+        ring.begin_late()
+    norm_blocks(9, 11)
     with jax.named_scope("wait_relay"):
-        for ring in in_2:
+        for ring in rest_a + own_b:
             ring.relay()
-    norm_blocks(13, 16)
-    with jax.named_scope("wait_in_2"):
-        for ring in in_own + in_2:
+    norm_blocks(11, 16)
+    with jax.named_scope("wait_relay_b"):
+        for ring in rest_b + out_1:
+            ring.relay()
+    with jax.named_scope("wait_in_a"):
+        for ring in own_a + rest_a:
             ring.near()
             ring.finish()
 
@@ -420,13 +445,21 @@
     def swapped(v):
         return jnp.where(low_half, pltpu.roll(v, 96, 1), pltpu.roll(v, 32, 1))
 
-    def project(s, starts):
+    def gate(s, starts):
         n = 256 // len(starts)
         at = [pl.ds(pl.multiple_of(s * T + r, 128), n) for r in starts]
         rows = jnp.concatenate([normed[rs, :] for rs in at], axis=0)
         a = dot(rows, w_a[...].reshape(D, 256))
         gated = a[:, :128] * jax.nn.sigmoid(a[:, 128:])
         gated = gated.astype(BF16).astype(F32)
+        for k in range(2):
+            r = pl.multiple_of(starts[k] if len(starts) == 2 else starts[0] + k * 128, 128)
+            gpad[s, pl.ds(RIM + r, 128), :] = gated[k * 128 : (k + 1) * 128]
+
+    def project(s, starts):
+        n = 256 // len(starts)
+        at = [pl.ds(pl.multiple_of(s * T + r, 128), n) for r in starts]
+        rows = jnp.concatenate([normed[rs, :] for rs in at], axis=0)
         b = dot(rows, w_b[...].reshape(D, 256))
         at = [pl.ds(pl.multiple_of(r, 128), n) for r in starts]
         cosine = jnp.concatenate([cos_ref[rs, :] for rs in at], axis=0)
@@ -442,7 +475,6 @@
         for k in range(2):
             r = pl.multiple_of(starts[k] if len(starts) == 2 else starts[0] + k * 128, 128)
             part = slice(k * 128, (k + 1) * 128)
-            gpad[s, pl.ds(RIM + r, 128), :] = gated[part]
             qz[s, r // 128, 0] = q_0[part]
             qz[s, r // 128, 1] = q_1[part]
             kpad[s, pl.ds(WINDOW + r, 128), :] = twice[part]
@@ -475,33 +507,53 @@
         start(conv_out_copies(s)[0])
         cbm[s, :, conv_lanes] = fsend[s, rows_of(tp), :]
 
+    def gate_edges(k, carry):
+        for s in (2 * k, 2 * k + 1):
+            gate(s, (0, T - 128))
+        for s in (2 * k, 2 * k + 1):
+            start(rims(s)[0])
+        return carry
+
     def project_edges(k, carry):
         for s in (2 * k, 2 * k + 1):
             project(s, (0, T - 128))
         for s in (2 * k, 2 * k + 1):
-            start(rims(s)[0])
-        for s in (2 * k, 2 * k + 1):
             start(edge_keys(s)[0])
         return carry
 
     inner = T // 256 - 1
 
+    def inner_rows(s, step):
+        lax.fori_loop(0, inner, lambda k, carry: step(s, (128 + k * 256,)) or carry, 0, unroll=inner)
+
+    def gate_inner(s, carry):
+        inner_rows(s, gate)
+        return carry
+
+    def each_convolve(s, carry):
+        convolve(s)
+        return carry
+
+    with jax.named_scope("gate_edges"):
+        lax.fori_loop(0, SEQS // 2, gate_edges, 0)
+    with jax.named_scope("gate_inner"):
+        lax.fori_loop(0, SEQS, gate_inner, 0)
+    with jax.named_scope("wait_out_1"):
+        for ring in out_1:
+            ring.near()
+            ring.finish()
+    for ring in out_2:
+        ring.begin_direct()
+    with jax.named_scope("wait_in_b"):
+        for ring in own_b + rest_b:
+            ring.near()
+            ring.finish()
     with jax.named_scope("project_edges"):
         lax.fori_loop(0, SEQS // 2, project_edges, 0)
-    with jax.named_scope("wait_out_1"):
-        for group in out_1:
-            arrived(group)
     for ring in out_2:
-        ring.begin()
+        ring.begin_late()
     start(pair_1[0])
-
-    def project_inner(s):
-        def step(k, carry):
-            project(s, (128 + k * 256,))
-            return carry
-
-        with jax.named_scope("project"):
-            lax.fori_loop(0, inner, step, 0, unroll=inner)
+    lax.fori_loop(0, SEQS, each_convolve, 0)
 
     head_lane = lax.broadcasted_iota(jnp.int32, (1, 256), 1)
     sink_row = jnp.where(head_lane < 128, sink[0], sink[1])
@@ -563,32 +615,24 @@
         bm[s, :, attn_lanes] = asend[s, rows_of(tp), :]
 
     def sequence(s, carry):
-        project_inner(s)
-
         @pl.when(s == SEQS - 1)
         def _():
-            with jax.named_scope("wait_out_2"):
+            with jax.named_scope("wait_out_near"):
                 for ring in out_2:
-                    ring.finish()
-            start(pair_4[0])
-
-        convolve(s)
-
-        @pl.when(s == min(1, SEQS - 1))
+                    ring.near()
+            if X > 2:
+                start(pair_3[0])
+
+        with jax.named_scope("project"):
+            inner_rows(s, project)
+
+        @pl.when(s == 0)
         def _():
             with jax.named_scope("wait_out_relay"):
                 for ring in out_2:
                     ring.relay()
             if X > 2:
                 start(pair_2[0])
-
-        @pl.when(s == min(2, SEQS - 1))
-        def _():
-            with jax.named_scope("wait_out_near"):
-                for ring in out_2:
-                    ring.near()
-            if X > 2:
-                start(pair_3[0])
 
         attend(s)
         return carry
@@ -616,74 +660,87 @@
         with jax.named_scope("channel_norm"):
             lax.fori_loop(0, 128 // 16, group, 0, unroll=8)
 
-    def out_columns(p, h):
-        zz, xx = p // (X // 2), (p % (X // 2)) * 2
+    def out_pair(blocks, h):
+        at = [((z + dz) % Z, (x + dx) % X) for dz, dx in blocks]
         pieces = [
-            jnp.concatenate([o_w[cc, hh, zz, xx], o_w[cc, hh, zz, xx + 1]], axis=1)
+            jnp.concatenate([o_w[cc, hh, zz, xx] for zz, xx in at], axis=1)
             for cc in range(CORES)
             for hh in h
         ]
-        return jnp.concatenate(pieces, axis=0)
-
-    columns_of = lambda p: pl.ds(pl.multiple_of(p * 256, 256), 256)
-    first_rows = SEQS // 2
-
+        columns = [pl.ds(pl.multiple_of((zz * X + xx) * 128, 128), 128) for zz, xx in at]
+        return jnp.concatenate(pieces, axis=0), columns
+
+    everything = [(dz, dx) for dz in range(Z) for dx in range(X)]
+    early = [k for k in everything if X > 2 and 2 not in k]
+    early = early[: len(early) // 2 * 2]
+    late = [k for k in everything if k not in early]
+    early, late = ([b[n : n + 2] for n in range(0, len(b), 2)] for b in (early, late))
+    branch = Y * 128
+    half = SEQS // 2
+
+    def rows_out(seqs, h):
+        first = [(2 * cc + h) * branch for cc in range(CORES)]
+        n = seqs.stop - seqs.start
+        lanes = [bm[seqs, :, k : k + branch].reshape(n * 128, branch) for k in first]
+        return jnp.concatenate(lanes, axis=1)
+
+    def out_conv(n, blocks):
+        acc = dot(rows_out(slice(0, SEQS), 0), out_pair(blocks, (0,))[0])
+        partial_out[n] = acc.reshape(SEQS, 128, 256)
+
+    def out_attn(n, blocks, seqs):
+        weights, columns = out_pair(blocks, (1,))
+        count = seqs.stop - seqs.start
+        acc = dot(rows_out(seqs, 1), weights).reshape(count, 128, 256) + partial_out[n, seqs]
+        acc = acc.astype(BF16)
+        for n in range(2):
+            mixed[seqs, :, columns[n]] = acc[:, :, n * 128 : (n + 1) * 128]
+
+    early = list(enumerate(early))
+    late = [(len(early) + n, blocks) for n, blocks in enumerate(late)]
     for s in range(SEQS):
         finish(s)
-        if s == first_rows - 1:
-            with jax.named_scope("wait_pair"):
-                for group in pairs:
-                    arrived(group)
-            with jax.named_scope("wait_attn"):
-                for n in range(first_rows):
-                    arrived(attn_out_copies(n))
-
-            def out_whole(p, carry):
-                rows = bm[:first_rows].reshape(first_rows * 128, TP * 256)
-                acc = dot(rows, out_columns(p, (0, 1)))
-                mixed[:first_rows, :, columns_of(p)] = acc.astype(BF16).reshape(first_rows, 128, 256)
-                return carry
-
-            with jax.named_scope("out_whole"):
-                lax.fori_loop(0, NSP // 2, out_whole, 0, unroll=2)
-
-    n_late = SEQS - first_rows
-    branch = Y * 128
-
-    def late_rows(h):
-        first = [(2 * cc + h) * branch for cc in range(CORES)]
-        lanes = [bm[first_rows:, :, k : k + branch].reshape(n_late * 128, branch) for k in first]
-        return jnp.concatenate(lanes, axis=1)
-
-    def out_conv(p, carry):
-        partial_out[p] = dot(late_rows(0), out_columns(p, (0,)))
-        return carry
-
+    with jax.named_scope("wait_pair"):
+        for group in pairs[:-1]:
+            arrived(group)
     with jax.named_scope("out_conv"):
-        lax.fori_loop(0, NSP // 2, out_conv, 0, unroll=2)
+        for n, blocks in early:
+            out_conv(n, blocks)
+    with jax.named_scope("wait_out_2"):
+        for ring in out_2:
+            ring.finish()
+    start(pair_4[0])
     with jax.named_scope("wait_attn"):
-        for n in range(first_rows, SEQS):
-            arrived(attn_out_copies(n))
-
-    def out_attn(p, carry):
-        acc = partial_out[p] + dot(late_rows(1), out_columns(p, (1,)))
-        mixed[first_rows:, :, columns_of(p)] = acc.astype(BF16).reshape(n_late, 128, 256)
-        return carry
-
+        for s in range(half):
+            arrived(attn_out_copies(s))
     with jax.named_scope("out_attn"):
-        lax.fori_loop(0, NSP // 2, out_attn, 0, unroll=2)
-
-    for group in in_1 + [gains] + out_0 + out_1 + pairs:
-        left_here(group)
-    for ring in in_own + in_2 + out_2:
-        ring.drain()
-
-    def drain(s, carry):
-        for group in (rims(s), edge_keys(s), conv_out_copies(s), attn_out_copies(s)):
-            left_here(group)
-        return carry
-
-    lax.fori_loop(0, SEQS, drain, 0)
+        for n, blocks in early:
+            out_attn(n, blocks, slice(0, half))
+    with jax.named_scope("wait_pair"):
+        arrived(pair_4)
+    with jax.named_scope("out_conv"):
+        for n, blocks in late:
+            out_conv(n, blocks)
+    with jax.named_scope("out_attn"):
+        for n, blocks in late:
+            out_attn(n, blocks, slice(0, half))
+    with jax.named_scope("wait_attn"):
+        for s in range(half, SEQS):
+            arrived(attn_out_copies(s))
+    with jax.named_scope("out_attn"):
+        for n, blocks in early + late:
+            out_attn(n, blocks, slice(half, SEQS))
+
+    rings = own_a + rest_a + own_b + rest_b + out_1 + out_2
+    groups = first_a + first_b + out_0 + pairs + [group for ring in rings for group in ring.groups()]
+    for s in range(SEQS):
+        groups += [rims(s), edge_keys(s), conv_out_copies(s), attn_out_copies(s)]
+    sent_rows = sum(group[2] for group in groups) // (2 * D)
+    gains[1].wait_send()
+    while sent_rows > 0:
+        gone = normed.at[pl.ds(0, min(sent_rows, SEQS * T))]
+        remote(gone, gone, 0, right).wait_send()
+        sent_rows -= SEQS * T
 
 
 def on_device(
@@ -710,7 +767,7 @@
     angles = np.concatenate(parts)[:, None] * np.tile(inverse.astype(np.float64), 4)[None, :]
     turns = np.stack([np.cos(angles), np.sin(angles)]).astype(np.float32)
 
-    n_copies = 2 + 24 + 2 + 2 + 1 + 12 + 4 + 4 * seqs
+    n_copies = 4 + 48 + 2 + 12 + 1 + 12 + 4 + 4 * seqs
     vmem = pl.BlockSpec(memory_space=pltpu.VMEM)
     far = pl.BlockSpec(memory_space=pl.ANY)
     call = pl.pallas_call(
@@ -745,14 +802,14 @@
             pltpu.VMEM((2, WINDOW, 256), F32),
             pltpu.VMEM((2, 3, WINDOW, 256), F32),
             pltpu.VMEM((2, 3, WINDOW, 256), BF16),
-            pltpu.VMEM((xs * zs // 2, seqs // 2 * 128, 256), F32),
+            pltpu.VMEM((xs * zs // 2, seqs, 128, 256), F32),
             pltpu.VMEM((seqs, toks, 128), BF16),
             pltpu.VMEM((seqs, toks, 128), BF16),
             pltpu.VMEM((seqs, toks // tps, tps * 128), BF16),
             pltpu.VMEM((seqs, toks // tps, tps * 256), BF16),
             pltpu.SemaphoreType.DMA((SLOTS,)),
             pltpu.SemaphoreType.DMA((12,)),
-            pltpu.SemaphoreType.DMA((n_copies,)),
+            pltpu.SemaphoreType.DMA((2,)),
             pltpu.SemaphoreType.DMA((n_copies,)),
         ],
         compiler_params=pltpu.CompilerParams(

time: 65.3 us -> 62.1 us (0.951)
  Pallas kernels: 62.6 us -> 59.4 us
    pallas_call x1, Pallas kernels: 62.6 us -> 59.4 us  [on_device(): call(tokens, norm_gain.reshape(-1, 128), conv_value_weight, conv_gate_wei...]
where the time goes in v3:
time: 62.1 us; the launch traced here: 62 us
  Pallas kernels  59.4 us (96%)
  local copies, waits for them, and re-layouts  1.94 us (3%)
  between operations  0.64 us (1%)
    pallas_call x1, Pallas kernels, on_device(): call(tokens, norm_gain.reshape(-1, 128), conv_value_weight, conv_gate_wei...  59.4 us
    unnamed x2, local copies, waits for them, and re-layouts  1.94 us

profile of v3, /device:TPU:1, one launch (start us, length us, event | category | flops | bytes accessed | tf_op | source)
XLA Modules:
  0.0 62.0 jit_solution(1710051035170734434)
XLA Ops:
  0.6 59.4 %layer.1 = (bf16[4,128,2048]{2,1,0:T(8,128)(2,1)S(1)}, f32[4,2,1024]{2,1,0:T(2,128)S(1)}) custom-call(bf16[4,1024,2048]{2,1,0:T(8,128)(2,1)} %tokens.1, bf16[16,128]{1,0:T(8,128)(2,1)} %bitcast.6, bf16[128,128]{1,0:T(8,128)(2,1)} %w_value.1, bf16[128,128]{1,0:T(8,128)(2,1)} %w_gate.1, bf16[128,128]{1,0:T(8,128)(2,1)} %w_query.1, bf16[64,128]{1,0:T(8,128)(2,1)} %bitcast.4, ...), custom_call_target="tpu_custom_call" | custom-call | tf_op jit(solution)/shard_map/layer/pallas_call | solution.py:820
  60.0 1.3 %copy.17 = bf16[4,128,2048]{2,1,0:T(8,128)(2,1)} copy(bf16[4,128,2048]{2,1,0:T(8,128)(2,1)S(1)} %get-tuple-element.2) | data formatting | bytes 4194304
  61.4 0.6 copy.18

commit v4 on v3

--- a/solution.py
+++ b/solution.py
@@ -244,7 +244,22 @@
         ]
         return first, own, rest
 
-    first_a, own_a, rest_a = gather_of(w_a)
+    def short_gather_of(w):
+        def send(f, blocks, at, size, whole):
+            pairs = [(ref, ref, at(d)) for k in blocks for ref in [half_block(w, f, k)] for d in range(1, size)]
+            return group_of(ids(1), pairs, whole)
+
+        def half_block(w, f, k):
+            at_zx = (z, (x + k) % X) if f == 0 else ((z + k) % Z, x)
+            return w.at[at_zx[0], at_zx[1], pl.ds(64 * f, 64)]
+
+        few, many = w.at[0, pl.ds(0, X - 1), pl.ds(0, 64)], w.at[pl.ds(0, Z - 1), pl.ds(0, X - 1), pl.ds(0, 64)]
+        first = [send(0, [0], at_x, X, few), send(1, [0], at_z, Z, few)]
+        own = [send(0, [0], at_z, Z, few), send(1, [0], at_x, X, few)]
+        rest = [send(0, range(1, X), at_z, Z, many), send(1, range(1, Z), at_x, X, many)]
+        return first, own, rest
+
+    first_a, own_a, rest_a = short_gather_of(w_a)
     first_b, own_b, rest_b = gather_of(w_b)
     own_gain = gain_all.at[slot]
     gains = group_of(ids(1), [(own_gain, own_gain, at_tp(d)) for d in range(1, TP)], gain_all.at[pl.ds(0, TP - 1)], 1)
@@ -335,10 +350,8 @@
         loads[n].wait()
     with jax.named_scope("greet"):
         pl.semaphore_wait(barrier, len(greeted))
-    for group in first_a:
+    for group in first_a + own_a:
         start(group[0])
-    for ring in own_a:
-        ring.begin()
 
     for n in (8, 9, 10):
         loads[n].wait()
@@ -360,6 +373,8 @@
 
     for n in (5, 6, 7):
         loads[n].wait()
+    loads[2].wait()
+    w_b[z, x, :, 0:128] = (w_b[z, x, :, 0:128].astype(F32) * HEAD_DIM**-0.5).astype(BF16)
     w_b[z, x, :, 128:256] = key_buf[...].astype(F32).T.astype(BF16)
     taps_buf[...] = taps_rows[...].astype(F32)
     for n in range(D // 128):
@@ -372,7 +387,7 @@
     query_i = lax.broadcasted_iota(jnp.int32, (WINDOW, 256), 1) % WINDOW
     bias[0] = jnp.where(key_i >= query_i, 0.0, MASK_VALUE)
     bias[1] = jnp.where(key_i <= query_i, 0.0, MASK_VALUE)
-    for n in range(2, 5):
+    for n in range(3, 5):
         loads[n].wait()
 
     def ln_block(i, carry):
@@ -405,20 +420,17 @@
     with jax.named_scope("wait_in_1"):
         for group in first_a:
             arrived(group)
-    for ring in rest_a:
-        ring.begin()
-    with jax.named_scope("wait_own"):
-        for ring in own_a:
-            ring.relay()
+    for group in rest_a:
+        start(group[0])
     for ring in own_b:
         ring.begin()
-    norm_blocks(5, 7)
+    norm_blocks(5, 9)
     with jax.named_scope("wait_in_b1"):
         for group in first_b:
             arrived(group)
     for ring in rest_b:
         ring.begin()
-    norm_blocks(7, 9)
+    norm_blocks(9, 11)
     with jax.named_scope("wait_out_0"):
         for group in out_0:
             arrived(group)
@@ -426,18 +438,10 @@
         ring.begin_direct()
     for ring in out_1:
         ring.begin_late()
-    norm_blocks(9, 11)
-    with jax.named_scope("wait_relay"):
-        for ring in rest_a + own_b:
-            ring.relay()
     norm_blocks(11, 16)
-    with jax.named_scope("wait_relay_b"):
-        for ring in rest_b + out_1:
-            ring.relay()
     with jax.named_scope("wait_in_a"):
-        for ring in own_a + rest_a:
-            ring.near()
-            ring.finish()
+        for group in own_a + rest_a:
+            arrived(group)
 
     lane = lax.broadcasted_iota(jnp.int32, (1, 128), 1)
     low_head = lane < HEAD_DIM
@@ -465,7 +469,7 @@
         cosine = jnp.concatenate([cos_ref[rs, :] for rs in at], axis=0)
         sine = jnp.concatenate([sin_ref[rs, :] for rs in at], axis=0)
         q, kv = b[:, :128], b[:, 128:]
-        q = (q * cosine + swapped(q) * sine) * (HEAD_DIM**-0.5)
+        q = q * cosine + swapped(q) * sine
         zero = jnp.zeros_like(q)
         q_0 = jnp.where(low_head, q, zero).astype(BF16)
         q_1 = jnp.where(low_head, zero, q).astype(BF16)
@@ -536,6 +540,9 @@
 
     with jax.named_scope("gate_edges"):
         lax.fori_loop(0, SEQS // 2, gate_edges, 0)
+    with jax.named_scope("wait_relay_b"):
+        for ring in own_b + rest_b + out_1:
+            ring.relay()
     with jax.named_scope("gate_inner"):
         lax.fori_loop(0, SEQS, gate_inner, 0)
     with jax.named_scope("wait_out_1"):
@@ -544,6 +551,7 @@
             ring.finish()
     for ring in out_2:
         ring.begin_direct()
+    lax.fori_loop(0, SEQS // 2, each_convolve, 0)
     with jax.named_scope("wait_in_b"):
         for ring in own_b + rest_b:
             ring.near()
@@ -553,7 +561,7 @@
     for ring in out_2:
         ring.begin_late()
     start(pair_1[0])
-    lax.fori_loop(0, SEQS, each_convolve, 0)
+    lax.fori_loop(SEQS // 2, SEQS, each_convolve, 0)
 
     head_lane = lax.broadcasted_iota(jnp.int32, (1, 256), 1)
     sink_row = jnp.where(head_lane < 128, sink[0], sink[1])
@@ -611,20 +619,27 @@
                     weigh(b - 1)
                 if b >= 2:
                     collect(b - 2)
+        @pl.when(s == SEQS - 1)
+        def _():
+            with jax.named_scope("wait_out_2"):
+                for ring in out_2:
+                    ring.finish()
+            start(pair_4[0])
+
         start(attn_out_copies(s)[0])
         bm[s, :, attn_lanes] = asend[s, rows_of(tp), :]
 
     def sequence(s, carry):
-        @pl.when(s == SEQS - 1)
+        with jax.named_scope("project"):
+            inner_rows(s, project)
+
+        @pl.when(s == SEQS - 2)
         def _():
             with jax.named_scope("wait_out_near"):
                 for ring in out_2:
                     ring.near()
             if X > 2:
                 start(pair_3[0])
-
-        with jax.named_scope("project"):
-            inner_rows(s, project)
 
         @pl.when(s == 0)
         def _():
@@ -706,10 +721,6 @@
     with jax.named_scope("out_conv"):
         for n, blocks in early:
             out_conv(n, blocks)
-    with jax.named_scope("wait_out_2"):
-        for ring in out_2:
-            ring.finish()
-    start(pair_4[0])
     with jax.named_scope("wait_attn"):
         for s in range(half):
             arrived(attn_out_copies(s))
@@ -731,8 +742,8 @@
         for n, blocks in early + late:
             out_attn(n, blocks, slice(half, SEQS))
 
-    rings = own_a + rest_a + own_b + rest_b + out_1 + out_2
-    groups = first_a + first_b + out_0 + pairs + [group for ring in rings for group in ring.groups()]
+    rings = own_b + rest_b + out_1 + out_2
+    groups = first_a + own_a + rest_a + first_b + out_0 + pairs + [group for ring in rings for group in ring.groups()]
     for s in range(SEQS):
         groups += [rims(s), edge_keys(s), conv_out_copies(s), attn_out_copies(s)]
     sent_rows = sum(group[2] for group in groups) // (2 * D)
@@ -767,7 +778,7 @@
     angles = np.concatenate(parts)[:, None] * np.tile(inverse.astype(np.float64), 4)[None, :]
     turns = np.stack([np.cos(angles), np.sin(angles)]).astype(np.float32)
 
-    n_copies = 4 + 48 + 2 + 12 + 1 + 12 + 4 + 4 * seqs
+    n_copies = 6 + 26 + 2 + 12 + 1 + 12 + 4 + 4 * seqs
     vmem = pl.BlockSpec(memory_space=pltpu.VMEM)
     far = pl.BlockSpec(memory_space=pl.ANY)
     call = pl.pallas_call(

time: 62.1 us -> 59.4 us (0.957)
  Pallas kernels: 59.4 us -> 56.7 us
    pallas_call x1, Pallas kernels: 59.4 us -> 56.7 us  [on_device(): call(tokens, norm_gain.reshape(-1, 128), conv_value_weight, conv_gate_wei...]
where the time goes in v4:
time: 59.4 us; the launch traced here: 59.2 us
  Pallas kernels  56.7 us (95%)
  local copies, waits for them, and re-layouts  1.94 us (3%)
  between operations  0.64 us (1%)
    pallas_call x1, Pallas kernels, on_device(): call(tokens, norm_gain.reshape(-1, 128), conv_value_weight, conv_gate_wei...  56.7 us
    unnamed x2, local copies, waits for them, and re-layouts  1.94 us

profile of v4, /device:TPU:1, one launch (start us, length us, event | category | flops | bytes accessed | tf_op | source)
XLA Modules:
  0.0 59.2 jit_solution(17726149156423674571)
XLA Ops:
  0.6 56.7 %layer.1 = (bf16[4,128,2048]{2,1,0:T(8,128)(2,1)S(1)}, f32[4,2,1024]{2,1,0:T(2,128)S(1)}) custom-call(bf16[4,1024,2048]{2,1,0:T(8,128)(2,1)} %tokens.1, bf16[16,128]{1,0:T(8,128)(2,1)} %bitcast.6, bf16[128,128]{1,0:T(8,128)(2,1)} %w_value.1, bf16[128,128]{1,0:T(8,128)(2,1)} %w_gate.1, bf16[128,128]{1,0:T(8,128)(2,1)} %w_query.1, bf16[64,128]{1,0:T(8,128)(2,1)} %bitcast.4, ...), custom_call_target="tpu_custom_call" | custom-call | tf_op jit(solution)/shard_map/layer/pallas_call | solution.py:831
  57.3 1.3 %copy.17 = bf16[4,128,2048]{2,1,0:T(8,128)(2,1)} copy(bf16[4,128,2048]{2,1,0:T(8,128)(2,1)S(1)} %get-tuple-element.2) | data formatting | bytes 4194304
  58.6 0.6 %copy.18 = f32[4,2,1024]{2,1,0:T(2,128)} copy(f32[4,2,1024]{2,1,0:T(2,128)S(1)} %get-tuple-element.3) | data formatting | bytes 65536

commit v5 on v4

--- a/solution.py
+++ b/solution.py
@@ -754,6 +754,16 @@
         sent_rows -= SEQS * T
 
 
+def put(mixed, log_total, mixed_out, log_out, sem):
+    seqs = mixed.shape[0]
+    copies = [pltpu.make_async_copy(log_total, log_out, sem.at[seqs])]
+    copies += [pltpu.make_async_copy(mixed.at[s], mixed_out.at[s], sem.at[s]) for s in range(seqs)]
+    for cp in copies:
+        cp.start()
+    for cp in copies:
+        cp.wait()
+
+
 def on_device(
     grid_shape,
     tokens,
@@ -828,7 +838,7 @@
         ),
         name="layer",
     )
-    return call(
+    mixed, log_total = call(
         tokens,
         norm_gain.reshape(-1, 128),
         conv_value_weight,
@@ -843,6 +853,15 @@
         out_attn_weight,
         jnp.asarray(turns),
     )
+    return pl.pallas_call(
+        put,
+        out_shape=(jax.ShapeDtypeStruct(mixed.shape, BF16), jax.ShapeDtypeStruct(log_total.shape, F32)),
+        in_specs=[far, far],
+        out_specs=(far, far),
+        scratch_shapes=[pltpu.SemaphoreType.DMA((seqs + 1,))],
+        compiler_params=pltpu.CompilerParams(vmem_limit_bytes=2**20),
+        name="put",
+    )(mixed, log_total)
 
 
 def solution(mesh):

time: 59.4 us -> 58.9 us (level)
  local copies, waits for them, and re-layouts: 1.94 us -> 0 us
  Pallas kernels: 56.7 us -> 58 us
    unnamed x2 -> x0, local copies, waits for them, and re-layouts: 1.94 us -> none
    pallas_call x0 -> x1, Pallas kernels: none -> 1.37 us  [on_device(): pl.pallas_call(put, out_shape=(jax.ShapeDtypeStruct(mixed.shape, BF16), j...]
where the time goes in v5:
time: 58.9 us; the launch traced here: 58.8 us
  Pallas kernels  58 us (98%)
  between operations  0.8 us (1%)
    pallas_call x1, Pallas kernels, on_device(): call(tokens, norm_gain.reshape(-1, 128), conv_value_weight, conv_gate_wei...  56.7 us
    pallas_call x1, Pallas kernels, on_device(): pl.pallas_call(put, out_shape=(jax.ShapeDtypeStruct(mixed.shape, BF16), j...  1.37 us

profile of v5, /device:TPU:1, one launch (start us, length us, event | category | flops | bytes accessed | tf_op | source)
XLA Modules:
  0.0 58.8 jit_solution(14063761330531261161)
XLA Ops:
  0.6 56.7 %layer.1 = (bf16[4,128,2048]{2,1,0:T(8,128)(2,1)S(1)}, f32[4,2,1024]{2,1,0:T(2,128)S(1)}) custom-call(bf16[4,1024,2048]{2,1,0:T(8,128)(2,1)} %tokens.1, bf16[16,128]{1,0:T(8,128)(2,1)} %bitcast.6, bf16[128,128]{1,0:T(8,128)(2,1)} %w_value.1, bf16[128,128]{1,0:T(8,128)(2,1)} %w_gate.1, bf16[128,128]{1,0:T(8,128)(2,1)} %w_query.1, bf16[64,128]{1,0:T(8,128)(2,1)} %bitcast.4, ...), custom_call_target="tpu_custom_call" | custom-call | tf_op jit(solution)/shard_map/layer/pallas_call | solution.py:841
  57.3 1.4 %put.1 = (bf16[4,128,2048]{2,1,0:T(8,128)(2,1)}, f32[4,2,1024]{2,1,0:T(2,128)}) custom-call(bf16[4,128,2048]{2,1,0:T(8,128)(2,1)S(1)} %get-tuple-element.4.mixed, f32[4,2,1024]{2,1,0:T(2,128)S(1)} %get-tuple-element.5.log_total), custom_call_target="tpu_custom_call" | custom-call | tf_op jit(solution)/shard_map/put/pallas_call | solution.py:856
